TPU v7x, 512 devices: a 8x2x16 block of a 8x16x16 slice. The times are simulated.
512 devices in a mesh: grp: 2 (over y), fs: 16 (over z), tp: 16 (over x, core).
Axes of the slice: x: 8, y: 2, z: 16, core: 2. Of those that a mesh axis runs over, the one named last changes fastest.
The devices are a block of a 8x16x16 slice.
Arguments:
- tokens: bfloat16 [16384, 2048], P(('grp', 'fs')), parts along dimension 0, may hold values from -6 to 6
- pre_gain: float32 [2048], replicated, may hold values from 0.1 to 1.9
- gate_weight: float32 [2048, 5632], P('fs', 'tp'), may hold values from -0.125 to 0.125
- gate_scale: float32 [5632], P('tp'), may hold values from 0.5 to 2
- up_weight: float32 [2048, 5632], P('fs', 'tp'), may hold values from -0.125 to 0.125
- up_scale: float32 [5632], P('tp'), may hold values from 0.5 to 2
- down_weight: float32 [5632, 2048], P('tp', 'fs'), may hold values from -0.078125 to 0.078125
- down_scale: float32 [2048], replicated, may hold values from 0.3 to 3
- post_gain: float32 [2048], replicated, may hold values from 0.1 to 1.9
Outputs:
- mixed: bfloat16 [16384, 2048], P(('grp', 'fs')), parts along dimension 0
There are 2 independent parts, one for each index of `grp`. A program takes and returns all parts, laid end to end along the dimension named above; an argument that names none is the same for every part. Nothing has to cross between parts.
All inputs are finite; a program needn't handle non-finite values.
Results may differ from a plain program's by a relative error of at most 0.018.
Values may be sent and summed in bfloat16 or wider, within the bound.
No kernel may reach another device: no remote copies, remote signals or barrier semaphores. Data moves between devices by JAX's collectives and lax.ppermute only.
A program may use at most 64 MiB of HBM per device.

v0:
```python
import jax
import jax.numpy as jnp
from jax import lax
from jax.sharding import PartitionSpec as P

EPS = 1e-06


def side_by_side(arrays, axis, dim, along):
    ends, at = ([], 0)
    for a in arrays[:-1]:
        at += a.shape[along]
        ends.append(at)
    both = jnp.concatenate(arrays, axis=along)
    return tuple(jnp.split(lax.all_gather(both, axis, axis=dim, tiled=True), ends, axis=along))


def from_everyone(array, axis):
    copies = jnp.broadcast_to(array, (lax.axis_size(axis), *array.shape))
    return lax.all_to_all(copies, axis, split_axis=0, concat_axis=0, tiled=True)


def joined_along(parts, dim):
    lengths = list(parts.shape[1:])
    lengths[dim] *= parts.shape[0]
    return jnp.moveaxis(parts, 0, dim).reshape(lengths)


def collect(array, axis, dim):
    parts = from_everyone(array, axis)
    return joined_along(parts, dim)


def cut_along(array, dim, count):
    lengths = array.shape
    parts = array.reshape(*lengths[:dim], count, lengths[dim] // count, *lengths[dim + 1 :])
    return jnp.moveaxis(parts, dim, 0)


def sent_and_summed(array, axis, dim):
    count = lax.axis_size(axis)
    parts = lax.all_to_all(cut_along(array, dim, count), axis, 0, 0, tiled=True)
    return jnp.sum(parts.astype(jnp.float32), axis=0)


def finish(summed, down_scale, post_gain):
    branch = summed * down_scale
    return (
        branch * lax.rsqrt(jnp.mean(branch * branch, axis=-1, keepdims=True) + EPS) * post_gain
    ).astype(jnp.bfloat16)


def body(
    tokens,
    pre_gain,
    gate_weight,
    gate_scale,
    up_weight,
    up_scale,
    down_weight,
    down_scale,
    post_gain,
):
    rows = tokens.astype(jnp.float32)
    normed = (
        rows * lax.rsqrt(jnp.mean(rows * rows, axis=-1, keepdims=True) + EPS) * pre_gain
    ).astype(jnp.bfloat16)
    gate_low = gate_weight.astype(jnp.bfloat16)
    up_low = up_weight.astype(jnp.bfloat16)
    down_low = down_weight.astype(jnp.bfloat16)
    gate_full, up_full = side_by_side((gate_low, up_low), "fs", 0, 1)
    gate = jnp.dot(normed, gate_full, preferred_element_type=jnp.float32) * gate_scale
    up = jnp.dot(normed, up_full, preferred_element_type=jnp.float32) * up_scale
    hidden = (jax.nn.silu(gate) * up).astype(jnp.bfloat16)
    down_full = collect(down_low, "fs", 1)
    summed = sent_and_summed(
        jnp.dot(hidden, down_full, preferred_element_type=jnp.float32).astype(jnp.bfloat16), "tp", 0
    )
    scaled = finish(summed, down_scale, post_gain)
    return lax.all_gather(scaled, "tp", axis=0, tiled=True)


def solution(mesh):
    in_specs = (
        P(("grp", "fs"), None),
        P(),
        P("fs", "tp"),
        P("tp"),
        P("fs", "tp"),
        P("tp"),
        P("tp", "fs"),
        P(),
        P(),
    )
    out_specs = P(("grp", "fs"), None)
    return jax.shard_map(body, mesh=mesh, in_specs=in_specs, out_specs=out_specs, check_vma=False)
```

profile of v0, /device:TPU:65, one launch (start us, length us, event | category | flops | bytes accessed | tf_op | source)
XLA Modules:
  0.0 292.3 jit_solution(8846115028078084117)
XLA Ops:
  6.5 0.0 all-gather.3.cloned.1.call-start
  6.6 0.9 convert_element_type.29
  7.5 0.9 convert_element_type.30
  8.4 0.7 pad_maximum_fusion
  9.1 0.1 all-gather.3.cloned.1.call-update
  9.2 0.9 convert_element_type.32
  10.1 0.0 copy-start
  10.1 1.3 broadcast_in_dim.2
  11.4 0.0 copy-start.3
  11.4 0.0 copy-start.4
  11.4 44.4 %all-to-all-start = ((bf16[16,352,128]{2,1,0:T(8,128)(2,1)}), bf16[16,352,128]{2,1,0:T(8,128)(2,1)S(1)}, u32[]{:S(2)}, u32[]{:S(2)}) async-start(bf16[16,352,128]{2,1,0:T(8,128)(2,1)} %broadcast_in_dim.2), calls=%async_computation | async-start | bytes 2883584 | tf_op jit(solution)/shard_map/all_to_all | solution.py:20
  55.8 0.1 all-gather.5.cloned.1.call-start
  55.9 0.0 copy-done
  55.9 0.5 fusion
  56.4 111.5 %all-gather.3.cloned.1.call-done = bf16[2048,704]{0,1:T(8,128)(2,1)} async-done(((bf16[128,704]{0,1:T(8,128)(2,1)}), bf16[2048,704]{0,1:T(8,128)(2,1)}) %all-gather.3.cloned.1.call-update) | async-done | bytes 2883600 | tf_op jit(solution)/shard_map/all_gather | solution.py:15
  167.8 0.0 copy-done.3
  167.8 0.0 copy-done.4
  167.8 3.2 %fusion.9 = f32[512,352]{0,1:T(8,128)} fusion(bf16[2048,704]{0,1:T(8,128)(2,1)} %all-gather.3.cloned.1.call-done, bf16[512,2048]{1,0:T(8,128)(2,1)S(1)} %copy-done, f32[2048]{0:T(1024)S(1)} %copy-done.3, f32[512]{0:T(512)S(1)} %add_rsqrt_fusion, f32[352]{0:T(512)S(1)} %copy-done.4), kind=kOutput, calls=%fused_computation.13 | convolution fusion | flops 742572032 | bytes 4271488 | tf_op jit(solution)/shard_map/dot_general | solution.py:72
  171.1 0.0 all-to-all-done
  171.1 5.2 %convolution_convert_fusion = bf16[512,2048]{1,0:T(8,128)(2,1)} fusion(bf16[2048,704]{0,1:T(8,128)(2,1)} %all-gather.3.cloned.1.call-done, f32[512,352]{0,1:T(8,128)} %fusion.9, bf16[512,2048]{1,0:T(8,128)(2,1)S(1)} %copy-done, f32[2048]{0:T(1024)S(1)} %copy-done.3, f32[512]{0:T(512)S(1)} %add_rsqrt_fusion, f32[352]{0:T(512)} %param.14, ...), kind=kOutput, calls=%fused_computation.6 | convolution fusion | flops 1482899456 | bytes 7811072 | tf_op jit(solution)/shard_map/dot_general | solution.py:77
  176.3 67.1 %all_to_all.10 = bf16[16,32,2048]{2,1,0:T(8,128)(2,1)S(1)} all-to-all(bf16[16,32,2048]{2,1,0:T(8,128)(2,1)} %bitcast.9), channel_id=1, replica_groups=mesh['grp'=2,'fs'=16,'tp'=16] {'tp'}, dimensions={0} | all-to-all | bytes 4194304 | tf_op jit(solution)/shard_map/all_to_all | solution.py:42
  243.4 0.0 copy-start.1
  243.4 0.0 copy-start.2
  243.4 0.4 convert_reduce_fusion
  243.8 0.3 copy-done.1
  244.1 0.1 multiply_reduce_fusion
  244.3 0.0 copy-done.2
  244.3 0.8 multiply_convert_fusion
  245.0 0.1 all-gather.5.cloned.1.call-update
  245.1 37.2 %all-gather.5.cloned.1.call-done = bf16[512,2048]{1,0:T(8,128)(2,1)} async-done(((bf16[32,2048]{1,0:T(8,128)(2,1)}), bf16[512,2048]{1,0:T(8,128)(2,1)}) %all-gather.5.cloned.1.call-update) | async-done | bytes 2097168 | tf_op jit(solution)/shard_map/all_gather | solution.py:80
  282.3 3.2 %copy.17 = bf16[512,2048]{1,0:T(8,128)(2,1)} copy(bf16[512,2048]{1,0:T(8,128)(2,1)} %all-gather.5.cloned.1.call-done) | data formatting | bytes 4194304
  (2 shorter events, 0.0 us)
Async XLA Ops:
  6.5 161.3 %all-gather.3.cloned.1.call-start = ((), (), s32[]{:S(2)}) async-start(), calls=%async_computation.2 | async-start | bytes 3063808 | tf_op jit(solution)/shard_map/all_gather | solution.py:15
  10.1 45.7 %copy-start = (bf16[512,2048]{1,0:T(8,128)(2,1)S(1)}, bf16[512,2048]{1,0:T(8,128)(2,1)}, u32[]{:S(2)}) copy-start(bf16[512,2048]{1,0:T(8,128)(2,1)} %param.9) | copy-start | bytes 6291460
  11.4 156.4 %copy-start.3 = (f32[2048]{0:T(1024)S(1)}, f32[2048]{0:T(1024)}, u32[]{:S(2)}) copy-start(f32[2048]{0:T(1024)} %param.10) | copy-start | bytes 24580
  11.4 156.4 %copy-start.4 = (f32[352]{0:T(512)S(1)}, f32[352]{0:T(512)}, u32[]{:S(2)}) copy-start(f32[352]{0:T(512)} %param.12) | copy-start | bytes 4228
  11.4 159.7 %all-to-all-start = ((bf16[16,352,128]{2,1,0:T(8,128)(2,1)}), bf16[16,352,128]{2,1,0:T(8,128)(2,1)S(1)}, u32[]{:S(2)}, u32[]{:S(2)}) async-start(bf16[16,352,128]{2,1,0:T(8,128)(2,1)} %broadcast_in_dim.2), calls=%async_computation | async-start | bytes 2883584 | tf_op jit(solution)/shard_map/all_to_all | solution.py:20
  55.8 226.5 %all-gather.5.cloned.1.call-start = ((), (), s32[]{:S(2)}) async-start(), calls=%async_computation.3 | async-start | bytes 2228224 | tf_op jit(solution)/shard_map/all_gather | solution.py:80
  243.4 0.7 copy-start.1
  243.4 0.8 copy-start.2
Sparse Core Ops, SparseCore 0:
  9.4 158.4 all-gather.2
  245.2 37.0 all-gather.4
where the time goes:
time: 293 us; the launch traced here: 292 us
  waiting for transfers between devices  149 us (51%)
  blocking collectives  67.1 us (23%)
  starting transfers between devices  44.4 us (15%)
  between operations  13.5 us (5%)
  matrix products  8.45 us (3%)
  other arithmetic  5.27 us (2%)
  local copies, waits for them, and re-layouts  4.77 us (2%)
    all_gather x1, waiting for transfers between devices, side_by_side(): lax.all_gather(both, axis, axis=dim, tiled=True)  111 us
    all_to_all x1, blocking collectives, sent_and_summed(): parts = lax.all_to_all(cut_along(array, dim, count), axis, 0, 0, tiled=True)  67.1 us
    all_to_all x1, starting transfers between devices, from_everyone(): return lax.all_to_all(copies, axis, split_axis=0, concat_axis=0, tiled=True)  44.4 us
    all_gather x1, waiting for transfers between devices, body(): return lax.all_gather(scaled, 'tp', axis=0, tiled=True)  37.2 us
  transfers between devices with their start and end apart: 3, of which 2 were waited for; matrix products, arithmetic and copies ran while one was open for 2% of the time, Pallas kernels for 0%

commit v1 on v0

v1 whole, which is shorter than its diff:
```python
import jax
import jax.numpy as jnp
from jax import lax
from jax.experimental import pallas as pl
from jax.experimental.pallas import tpu as pltpu
from jax.sharding import PartitionSpec as P

EPS = 1e-06
LANES = 128
CORES = 2
ROWS = 128


def flat(z, t, n_fs, n_tp):
    return (z % n_fs) * n_tp + t


def patterns(n_fs, n_tp):
    enter, own, ring = ([], [], [])
    for z in range(n_fs):
        for t in range(n_tp):
            here = flat(z, t, n_fs, n_tp)
            if t % CORES == 0:
                enter.append((here, flat(z, t + 1, n_fs, n_tp)))
                own.append((here, flat(z + 1, t, n_fs, n_tp)))
                ring.append((here, flat(z + 1, t, n_fs, n_tp)))
            else:
                enter.append((here, flat(z + 1, t - 1, n_fs, n_tp)))
                ring.append((here, flat(z - 1, t, n_fs, n_tp)))
    return enter, own, ring


def finish_kernel(n_fs, place, mine, other, scale, gain, out):
    z, core = (place[0], place[1])
    slots = mine.shape[1] // LANES
    total = None
    branches = []
    for held, which in ((mine, core), (other, 1 - core)):
        for k in range(slots):
            slab = lax.rem(jnp.where(which == 0, z - 1 - k, z + k) + n_fs, n_fs)
            branch = held[:, k * LANES : (k + 1) * LANES].astype(jnp.float32) * scale[pl.ds(slab, 1), :]
            squares = branch * branch
            total = squares if total is None else total + squares
            branches.append((slab, branch))
    width = LANES * len(branches)
    norm = lax.rsqrt(jnp.sum(total, axis=-1, keepdims=True) / width + EPS)
    for slab, branch in branches:
        at = pl.multiple_of(slab * LANES, LANES)
        out[:, pl.ds(at, LANES)] = (branch * norm * gain[pl.ds(slab, 1), :]).astype(out.dtype)


def finish(place, mine, other, down_scale, post_gain, n_fs):
    rows, half = mine.shape
    block = pl.BlockSpec((ROWS, half), lambda i, place: (i, 0))
    vector = pl.BlockSpec((2 * half // LANES, LANES), lambda i, place: (0, 0))
    return pl.pallas_call(
        lambda *refs: finish_kernel(n_fs, *refs),
        grid_spec=pltpu.PrefetchScalarGridSpec(
            num_scalar_prefetch=1,
            grid=(rows // ROWS,),
            in_specs=[block, block, vector, vector],
            out_specs=pl.BlockSpec((ROWS, 2 * half), lambda i, place: (i, 0)),
        ),
        out_shape=jax.ShapeDtypeStruct((rows, 2 * half), jnp.bfloat16),
    )(place, mine, other, down_scale.reshape(-1, LANES), post_gain.reshape(-1, LANES))


def body(
    tokens,
    pre_gain,
    gate_weight,
    gate_scale,
    up_weight,
    up_scale,
    down_weight,
    down_scale,
    post_gain,
):
    n_fs, n_tp = (lax.axis_size("fs"), lax.axis_size("tp"))
    both = ("fs", "tp")
    z, t = (lax.axis_index("fs"), lax.axis_index("tp"))
    core = t % CORES
    enter, own_first, ring = patterns(n_fs, n_tp)
    partner = [(i, i ^ 1) for i in range(n_tp)]
    chips = [[x * CORES + c for x in range(n_tp // CORES)] for c in range(CORES)]
    n_chips = n_tp // CORES
    low = jnp.bfloat16
    units = gate_weight.shape[1]

    packed = jnp.concatenate(
        [gate_weight.astype(low).T, up_weight.astype(low).T, down_weight.astype(low)], axis=0
    )
    other0 = lax.ppermute(packed, both, enter)
    shifted = lax.ppermute(packed, both, own_first)
    own0 = jnp.where(core == 0, shifted, packed)

    rows = tokens.astype(jnp.float32)
    inverse = lax.rsqrt(jnp.mean(rows * rows, axis=-1, keepdims=True) + EPS)

    def normed_slab(k):
        slab = jnp.where(core == 0, z - 1 - k, z + k) % n_fs
        part = lax.dynamic_slice_in_dim(tokens, slab * LANES, LANES, axis=1).astype(jnp.float32)
        return (part * inverse * lax.dynamic_slice_in_dim(pre_gain, slab * LANES, LANES)).astype(low)

    def product(weights, k_normed):
        return lax.dot_general(
            weights, k_normed, (((1,), (1,)), ((), ())), preferred_element_type=jnp.float32
        )

    first_own, first_other = (own0[: 2 * units], other0[: 2 * units])
    down = jnp.concatenate([own0[2 * units :], other0[2 * units :]], axis=0)
    downs = [down]
    slab = normed_slab(0)
    sum_own, sum_other = (product(first_own, slab), product(first_other, slab))
    for k in range(1, n_fs // 2):
        first_own = lax.ppermute(first_own, both, ring)
        first_other = lax.ppermute(first_other, both, ring)
        down = lax.ppermute(down, both, ring)
        downs.append(down)
        slab = normed_slab(k)
        sum_other = sum_other + product(first_other, slab)
        sum_own = sum_own + product(first_own, slab)

    arrived = lax.ppermute(sum_other.astype(low), "tp", partner)
    sums = sum_own + arrived.astype(jnp.float32)
    gate = sums[:units] * gate_scale[:, None]
    up = sums[units:] * up_scale[:, None]
    hidden = (jax.nn.silu(gate) * up).astype(low)
    hidden = jnp.concatenate([hidden, lax.ppermute(hidden, "tp", partner)], axis=0)

    columns = jnp.concatenate(downs, axis=1)
    partial = lax.dot_general(
        hidden, columns, (((0,), (0,)), ((), ())), preferred_element_type=jnp.float32
    ).astype(low)
    n_rows, half = partial.shape
    parts = lax.all_to_all(
        partial.reshape(n_chips, n_rows // n_chips, half),
        "tp", 0, 0, axis_index_groups=chips, tiled=True,
    )
    summed = jnp.sum(parts.astype(jnp.float32), axis=0).astype(low)
    mine = lax.all_to_all(
        jnp.broadcast_to(summed, (n_chips, *summed.shape)),
        "tp", 0, 0, axis_index_groups=chips, tiled=True,
    ).reshape(n_rows, half)
    other = lax.ppermute(mine, "tp", partner)
    place = jnp.stack([z, core]).astype(jnp.int32)
    return finish(place, mine, other, down_scale, post_gain, n_fs)


def solution(mesh):
    in_specs = (
        P(("grp", "fs"), None),
        P(),
        P("fs", "tp"),
        P("tp"),
        P("fs", "tp"),
        P("tp"),
        P("tp", "fs"),
        P(),
        P(),
    )
    out_specs = P(("grp", "fs"), None)
    return jax.shard_map(body, mesh=mesh, in_specs=in_specs, out_specs=out_specs, check_vma=False)
```

time: 293 us -> 229 us (0.78)
  waiting for transfers between devices: 149 us -> 17.4 us
  starting transfers between devices: 44.4 us -> 129 us
  between operations: 13.5 us -> 0.9 us
  blocking collectives: 67.1 us -> 60.3 us
  Pallas kernels: 0 us -> 5.07 us
  local copies, waits for them, and re-layouts: 4.77 us -> 1.63 us
    all_gather x2 -> x0, waiting for transfers between devices: 149 us -> none  [the longest x1 111 us: side_by_side(): lax.all_gather(both, axis, axis=dim, tiled=True)]
    ppermute x0 -> x26, starting transfers between devices: none -> 129 us  [the longest x7 54.3 us: body(): first_own = lax.ppermute(first_own, both, ring)]
    all_to_all x1 -> x0, starting transfers between devices: 44.4 us -> none  [from_everyone(): return lax.all_to_all(copies, axis, split_axis=0, concat_axis=0, tiled=True)]
    ppermute x0 -> x26, waiting for transfers between devices: none -> 17.4 us  [the longest x7 6.11 us: body(): first_other = lax.ppermute(first_other, both, ring)]
    all_to_all x1 -> x2, blocking collectives: 67.1 us -> 60.3 us  [the longest x1 32.6 us: body(): lax.all_to_all(partial.reshape(n_chips, n_rows // n_chips, half), 'tp', 0...]
    pallas_call x0 -> x1, Pallas kernels: none -> 5.07 us  [finish(): pl.pallas_call(lambda *refs: finish_kernel(n_fs, *refs), grid_spec=pltpu....]
    dot_general x2 -> x17, matrix products: 8.45 us -> 8.32 us  [the longest x16 7.32 us: product(): lax.dot_general(weights, k_normed, (((1,), (1,)), ((), ())), preferred_el...]
  transfers between devices with their start and end apart: 3 -> 26, of which waited for: 2 -> 7; matrix products, arithmetic and copies ran while one was open for 2% -> 5% of each run, Pallas kernels for 0% -> 0%
where the time goes in v1:
time: 229 us; the launch traced here: 228 us
  starting transfers between devices  129 us (56%)
  blocking collectives  60.3 us (26%)
  waiting for transfers between devices  17.4 us (8%)
  matrix products  8.32 us (4%)
  other arithmetic  5.24 us (2%)
  Pallas kernels  5.07 us (2%)
    ppermute x7, starting transfers between devices, body(): first_own = lax.ppermute(first_own, both, ring)  54.3 us
    all_to_all x1, blocking collectives, body(): lax.all_to_all(partial.reshape(n_chips, n_rows // n_chips, half), 'tp', 0...  32.6 us
    all_to_all x1, blocking collectives, body(): lax.all_to_all(jnp.broadcast_to(summed, (n_chips, *summed.shape)), 'tp',...  27.7 us
    ppermute x7, starting transfers between devices, body(): first_other = lax.ppermute(first_other, both, ring)  24.6 us
    ppermute x1, starting transfers between devices, body(): arrived = lax.ppermute(sum_other.astype(low), 'tp', partner)  16.9 us
    ppermute x7, starting transfers between devices, body(): down = lax.ppermute(down, both, ring)  13.7 us
    dot_general x16, matrix products, product(): lax.dot_general(weights, k_normed, (((1,), (1,)), ((), ())), preferred_el...  7.32 us
    ppermute x1, starting transfers between devices, body(): other = lax.ppermute(mine, 'tp', partner)  7.01 us
  transfers between devices with their start and end apart: 26, of which 7 were waited for; matrix products, arithmetic and copies ran while one was open for 5% of the time, Pallas kernels for 0%

profile of v1, /device:TPU:65, one launch (start us, length us, event | category | flops | bytes accessed | tf_op | source)
XLA Modules:
  0.0 227.5 jit_solution(1454541233129565218)
XLA Ops:
  0.0 0.9 convert_element_type.76
  0.9 1.0 convert_bitcast_fusion
  2.0 5.2 %collective-permute-start.8 = (bf16[1056,128]{1,0:T(8,128)(2,1)S(1)}, bf16[1056,128]{1,0:T(8,128)(2,1)S(1)}, u32[]{:S(2)}, u32[]{:S(2)}) collective-permute-start(bf16[1056,128]{1,0:T(8,128)(2,1)S(1)} %pad_maximum_fusion), channel_id=1, source_target_pairs={{0,1},{1,16},{2,3},{3,18},{4,5},{5,20},{6,7},{7,22},{8,9},{9,24},{... | collective-permute-start | bytes 811016 | tf_op jit(solution)/shard_map/ppermute | solution.py:93
  7.2 0.7 collective-permute-start
  7.9 2.1 multiply_reduce_fusion
  10.3 40.9 %collective-permute-start.1 = (bf16[704,128]{1,0:T(8,128)(2,1)S(1)}, bf16[704,128]{1,0:T(8,128)(2,1)S(1)}, u32[]{:S(2)}, u32[]{:S(2)}) collective-permute-start(bf16[704,128]{1,0:T(8,128)(2,1)S(1)} %slice.24), channel_id=1, source_target_pairs={{0,16},{1,241},{2,18},{3,243},{4,20},{5,245},{6,22},{7,247},{8,24}... | collective-permute-start | bytes 540680 | tf_op jit(solution)/shard_map/ppermute | solution.py:116
  51.4 2.5 %collective-permute-start.9 = (bf16[704,128]{1,0:T(8,128)(2,1)S(1)}, bf16[704,128]{1,0:T(8,128)(2,1)S(1)}, u32[]{:S(2)}, u32[]{:S(2)}) collective-permute-start(bf16[704,128]{1,0:T(8,128)(2,1)S(1)} %slice.25), channel_id=1, source_target_pairs={{0,16},{1,241},{2,18},{3,243},{4,20},{5,245},{6,22},{7,247},{8,24}... | collective-permute-start | bytes 540680 | tf_op jit(solution)/shard_map/ppermute | solution.py:117
  54.0 2.0 collective-permute-start.18
  56.0 2.7 %collective-permute-start.2 = (bf16[704,128]{1,0:T(8,128)(2,1)S(1)}, bf16[704,128]{1,0:T(8,128)(2,1)S(1)}, u32[]{:S(2)}, u32[]{:S(2)}) collective-permute-start(bf16[704,128]{1,0:T(8,128)(2,1)S(1)} %collective-permute-done.1), channel_id=1, source_target_pairs={{0,16},{1,241},{2,18},{3,243},{4,20},{5,245},{6,22},{7,247},{8,24}... | collective-permute-start | bytes 540680 | tf_op jit(solution)/shard_map/ppermute | solution.py:116
  59.7 2.0 collective-permute-start.10
  62.1 2.0 collective-permute-start.19
  64.6 1.4 collective-permute-done.10
  66.0 3.1 %collective-permute-start.11 = (bf16[704,128]{1,0:T(8,128)(2,1)S(1)}, bf16[704,128]{1,0:T(8,128)(2,1)S(1)}, u32[]{:S(2)}, u32[]{:S(2)}) collective-permute-start(bf16[704,128]{1,0:T(8,128)(2,1)S(1)} %collective-permute-done.10), channel_id=1, source_target_pairs={{0,16},{1,241},{2,18},{3,243},{4,20},{5,245},{6,22},{7,247},{8,24}... | collective-permute-start | bytes 540680 | tf_op jit(solution)/shard_map/ppermute | solution.py:117
  69.1 2.0 collective-permute-start.3
  71.1 2.0 collective-permute-start.20
  73.0 0.5 convolution_add_fusion.5
  74.0 2.5 %collective-permute-start.12 = (bf16[704,128]{1,0:T(8,128)(2,1)S(1)}, bf16[704,128]{1,0:T(8,128)(2,1)S(1)}, u32[]{:S(2)}, u32[]{:S(2)}) collective-permute-start(bf16[704,128]{1,0:T(8,128)(2,1)S(1)} %collective-permute-done.11), channel_id=1, source_target_pairs={{0,16},{1,241},{2,18},{3,243},{4,20},{5,245},{6,22},{7,247},{8,24}... | collective-permute-start | bytes 540680 | tf_op jit(solution)/shard_map/ppermute | solution.py:117
  76.6 2.0 collective-permute-start.4
  78.5 2.0 collective-permute-start.21
  80.5 0.5 convolution_add_fusion.4
  81.5 2.5 %collective-permute-start.13 = (bf16[704,128]{1,0:T(8,128)(2,1)S(1)}, bf16[704,128]{1,0:T(8,128)(2,1)S(1)}, u32[]{:S(2)}, u32[]{:S(2)}) collective-permute-start(bf16[704,128]{1,0:T(8,128)(2,1)S(1)} %collective-permute-done.12), channel_id=1, source_target_pairs={{0,16},{1,241},{2,18},{3,243},{4,20},{5,245},{6,22},{7,247},{8,24}... | collective-permute-start | bytes 540680 | tf_op jit(solution)/shard_map/ppermute | solution.py:117
  84.0 2.0 collective-permute-start.5
  86.0 2.0 collective-permute-start.22
  88.0 0.5 convolution_add_fusion.3
  88.4 3.0 %collective-permute-start.14 = (bf16[704,128]{1,0:T(8,128)(2,1)S(1)}, bf16[704,128]{1,0:T(8,128)(2,1)S(1)}, u32[]{:S(2)}, u32[]{:S(2)}) collective-permute-start(bf16[704,128]{1,0:T(8,128)(2,1)S(1)} %collective-permute-done.13), channel_id=1, source_target_pairs={{0,16},{1,241},{2,18},{3,243},{4,20},{5,245},{6,22},{7,247},{8,24}... | collective-permute-start | bytes 540680 | tf_op jit(solution)/shard_map/ppermute | solution.py:117
  91.5 0.5 convolution_add_fusion.2
  92.0 2.8 %collective-permute-done.14 = bf16[704,128]{1,0:T(8,128)(2,1)S(1)} collective-permute-done((bf16[704,128]{1,0:T(8,128)(2,1)S(1)}, bf16[704,128]{1,0:T(8,128)(2,1)S(1)}, u32[]{:S(2)}, u32[]{:S(2)}) %collective-permute-start.14) | collective-permute-done | bytes 180256 | tf_op jit(solution)/shard_map/ppermute | solution.py:117
  94.7 9.0 %collective-permute-start.15 = (bf16[704,128]{1,0:T(8,128)(2,1)S(1)}, bf16[704,128]{1,0:T(8,128)(2,1)S(1)}, u32[]{:S(2)}, u32[]{:S(2)}) collective-permute-start(bf16[704,128]{1,0:T(8,128)(2,1)S(1)} %collective-permute-done.14), channel_id=1, source_target_pairs={{0,16},{1,241},{2,18},{3,243},{4,20},{5,245},{6,22},{7,247},{8,24}... | collective-permute-start | bytes 540680 | tf_op jit(solution)/shard_map/ppermute | solution.py:117
  103.7 0.5 convolution_add_fusion.1
  104.2 1.9 collective-permute-done.15
  106.6 16.9 %collective-permute-start.16 = (bf16[704,512]{1,0:T(8,128)(2,1)S(1)}, bf16[704,512]{1,0:T(8,128)(2,1)S(1)}, u32[]{:S(2)}, u32[]{:S(2)}) collective-permute-start(bf16[704,512]{1,0:T(8,128)(2,1)S(1)} %fusion.1), channel_id=1, source_target_pairs={{0,1},{1,0},{2,3},{3,2},{4,5},{5,4},{6,7},{7,6},{8,9},{9,8},{10,11... | collective-permute-start | bytes 2162696 | tf_op jit(solution)/shard_map/ppermute | solution.py:124
  123.9 2.0 collective-permute-start.6
  125.9 2.0 collective-permute-start.23
  128.3 2.2 collective-permute-done.6
  130.5 2.9 %collective-permute-start.7 = (bf16[704,128]{1,0:T(8,128)(2,1)S(1)}, bf16[704,128]{1,0:T(8,128)(2,1)S(1)}, u32[]{:S(2)}, u32[]{:S(2)}) collective-permute-start(bf16[704,128]{1,0:T(8,128)(2,1)S(1)} %collective-permute-done.6), channel_id=1, source_target_pairs={{0,16},{1,241},{2,18},{3,243},{4,20},{5,245},{6,22},{7,247},{8,24}... | collective-permute-start | bytes 540680 | tf_op jit(solution)/shard_map/ppermute | solution.py:116
  133.4 0.5 convolution_add_fusion.8
  133.9 2.9 %collective-permute-done.7 = bf16[704,128]{1,0:T(8,128)(2,1)S(1)} collective-permute-done((bf16[704,128]{1,0:T(8,128)(2,1)S(1)}, bf16[704,128]{1,0:T(8,128)(2,1)S(1)}, u32[]{:S(2)}, u32[]{:S(2)}) %collective-permute-start.7) | collective-permute-done | bytes 180256 | tf_op jit(solution)/shard_map/ppermute | solution.py:116
  137.5 6.4 %collective-permute-start.17 = (bf16[352,512]{1,0:T(8,128)(2,1)S(1)}, bf16[352,512]{1,0:T(8,128)(2,1)S(1)}, u32[]{:S(2)}, u32[]{:S(2)}) collective-permute-start(bf16[352,512]{1,0:T(8,128)(2,1)S(1)} %fusion.3), channel_id=1, source_target_pairs={{0,1},{1,0},{2,3},{3,2},{4,5},{5,4},{6,7},{7,6},{8,9},{9,8},{10,11... | collective-permute-start | bytes 1081352 | tf_op jit(solution)/shard_map/ppermute | solution.py:129
  144.0 2.0 collective-permute-start.24
  146.1 4.5 %collective-permute-done.24 = bf16[704,128]{1,0:T(8,128)(2,1)S(1)} collective-permute-done((bf16[704,128]{1,0:T(8,128)(2,1)S(1)}, bf16[704,128]{1,0:T(8,128)(2,1)S(1)}, u32[]{:S(2)}, u32[]{:S(2)}) %collective-permute-start.24) | collective-permute-done | bytes 180256 | tf_op jit(solution)/shard_map/ppermute | solution.py:118
  150.6 1.0 convolution_convert_fusion
  151.6 32.6 %all_to_all.10 = bf16[8,64,1024]{2,1,0:T(8,128)(2,1)S(1)} all-to-all(bf16[8,64,1024]{2,1,0:T(8,128)(2,1)S(1)} %bitcast.27), channel_id=1, replica_groups={{0,2,4,6,8,10,12,14},{1,3,5,7,9,11,13,15},{16,18,20,22,24,26,28,30},{17..., dimensions={0} | all-to-all | bytes 2097152 | tf_op jit(solution)/shard_map/all_to_all | solution.py:136
  184.5 27.7 %all_to_all.11 = bf16[8,64,1024]{2,1,0:T(8,128)(2,1)S(1)} all-to-all(bf16[8,64,1024]{2,1,0:T(8,128)(2,1)S(1)} %broadcast_in_dim.2), channel_id=1, replica_groups={{0,2,4,6,8,10,12,14},{1,3,5,7,9,11,13,15},{16,18,20,22,24,26,28,30},{17..., dimensions={0} | all-to-all | bytes 2097152 | tf_op jit(solution)/shard_map/all_to_all | solution.py:141
  212.2 7.0 %collective-permute-start.25 = (bf16[512,1024]{1,0:T(8,128)(2,1)S(1)}, bf16[512,1024]{1,0:T(8,128)(2,1)S(1)}, u32[]{:S(2)}, u32[]{:S(2)}) collective-permute-start(bf16[512,1024]{1,0:T(8,128)(2,1)S(1)} %bitcast.25), channel_id=1, source_target_pairs={{0,1},{1,0},{2,3},{3,2},{4,5},{5,4},{6,7},{7,6},{8,9},{9,8},{10,11... | collective-permute-start | bytes 3145736 | tf_op jit(solution)/shard_map/ppermute | solution.py:145
  219.2 0.6 pad_add_fusion.refs_0_
  219.8 1.7 collective-permute-done.25.refs_2_
  221.5 0.9 copy-done.2
  222.5 5.1 %shard_map.91 = bf16[512,2048]{1,0:T(8,128)(2,1)} custom-call(s32[2]{0:T(128)} %pad_add_fusion.refs_0_, bf16[512,1024]{1,0:T(8,128)(2,1)} %bitcast.26, bf16[512,1024]{1,0:T(8,128)(2,1)} %copy-done.2, f32[16,128]{1,0:T(8,128)} %bitcast.28, f32[16,128]{1,0:T(8,128)} %bitcast.29), custom_call_target="tpu_custom_call" | custom-call | tf_op jit(solution)/shard_map/pallas_call | solution.py:56
  (59 shorter events, 5.9 us)
Async XLA Ops:
  2.0 49.2 %copy-start.5 = (f32[2048]{0:T(1024)S(1)}, f32[2048]{0:T(1024)}, u32[]{:S(2)}) copy-start(f32[2048]{0:T(1024)} %param.10) | copy-start | bytes 24580
  2.0 49.4 %collective-permute-start.8 = (bf16[1056,128]{1,0:T(8,128)(2,1)S(1)}, bf16[1056,128]{1,0:T(8,128)(2,1)S(1)}, u32[]{:S(2)}, u32[]{:S(2)}) collective-permute-start(bf16[1056,128]{1,0:T(8,128)(2,1)S(1)} %pad_maximum_fusion), channel_id=1, source_target_pairs={{0,1},{1,16},{2,3},{3,18},{4,5},{5,20},{6,7},{7,22},{8,9},{9,24},{... | collective-permute-start | bytes 811016 | tf_op jit(solution)/shard_map/ppermute | solution.py:93
  7.2 3.0 %collective-permute-start = (bf16[1056,128]{1,0:T(8,128)(2,1)S(1)}, bf16[1056,128]{1,0:T(8,128)(2,1)S(1)}, u32[]{:S(2)}, u32[]{:S(2)}) collective-permute-start(bf16[1056,128]{1,0:T(8,128)(2,1)S(1)} %pad_maximum_fusion), channel_id=1, source_target_pairs={{0,16},{2,18},{4,20},{6,22},{8,24},{10,26},{12,28},{14,30},{16,32}... | collective-permute-start | bytes 811016 | tf_op jit(solution)/shard_map/ppermute | solution.py:94
  9.9 48.8 %copy-start = (bf16[512,2048]{1,0:T(8,128)(2,1)S(1)}, bf16[512,2048]{1,0:T(8,128)(2,1)}, u32[]{:S(2)}) copy-start(bf16[512,2048]{1,0:T(8,128)(2,1)} %param.9) | copy-start | bytes 6291460
  10.3 45.7 %collective-permute-start.1 = (bf16[704,128]{1,0:T(8,128)(2,1)S(1)}, bf16[704,128]{1,0:T(8,128)(2,1)S(1)}, u32[]{:S(2)}, u32[]{:S(2)}) collective-permute-start(bf16[704,128]{1,0:T(8,128)(2,1)S(1)} %slice.24), channel_id=1, source_target_pairs={{0,16},{1,241},{2,18},{3,243},{4,20},{5,245},{6,22},{7,247},{8,24}... | collective-permute-start | bytes 540680 | tf_op jit(solution)/shard_map/ppermute | solution.py:116
  51.4 8.3 %collective-permute-start.9 = (bf16[704,128]{1,0:T(8,128)(2,1)S(1)}, bf16[704,128]{1,0:T(8,128)(2,1)S(1)}, u32[]{:S(2)}, u32[]{:S(2)}) collective-permute-start(bf16[704,128]{1,0:T(8,128)(2,1)S(1)} %slice.25), channel_id=1, source_target_pairs={{0,16},{1,241},{2,18},{3,243},{4,20},{5,245},{6,22},{7,247},{8,24}... | collective-permute-start | bytes 540680 | tf_op jit(solution)/shard_map/ppermute | solution.py:117
  54.0 8.1 %collective-permute-start.18 = (bf16[704,128]{1,0:T(8,128)(2,1)S(1)}, bf16[704,128]{1,0:T(8,128)(2,1)S(1)}, u32[]{:S(2)}, u32[]{:S(2)}) collective-permute-start(bf16[704,128]{1,0:T(8,128)(2,1)S(1)} %get-tuple-element.5), channel_id=1, source_target_pairs={{0,16},{1,241},{2,18},{3,243},{4,20},{5,245},{6,22},{7,247},{8,24}... | collective-permute-start | bytes 540680 | tf_op jit(solution)/shard_map/ppermute | solution.py:118
  56.0 13.1 %collective-permute-start.2 = (bf16[704,128]{1,0:T(8,128)(2,1)S(1)}, bf16[704,128]{1,0:T(8,128)(2,1)S(1)}, u32[]{:S(2)}, u32[]{:S(2)}) collective-permute-start(bf16[704,128]{1,0:T(8,128)(2,1)S(1)} %collective-permute-done.1), channel_id=1, source_target_pairs={{0,16},{1,241},{2,18},{3,243},{4,20},{5,245},{6,22},{7,247},{8,24}... | collective-permute-start | bytes 540680 | tf_op jit(solution)/shard_map/ppermute | solution.py:116
  59.7 6.3 %collective-permute-start.10 = (bf16[704,128]{1,0:T(8,128)(2,1)S(1)}, bf16[704,128]{1,0:T(8,128)(2,1)S(1)}, u32[]{:S(2)}, u32[]{:S(2)}) collective-permute-start(bf16[704,128]{1,0:T(8,128)(2,1)S(1)} %collective-permute-done.9), channel_id=1, source_target_pairs={{0,16},{1,241},{2,18},{3,243},{4,20},{5,245},{6,22},{7,247},{8,24}... | collective-permute-start | bytes 540680 | tf_op jit(solution)/shard_map/ppermute | solution.py:117
  62.1 9.0 %collective-permute-start.19 = (bf16[704,128]{1,0:T(8,128)(2,1)S(1)}, bf16[704,128]{1,0:T(8,128)(2,1)S(1)}, u32[]{:S(2)}, u32[]{:S(2)}) collective-permute-start(bf16[704,128]{1,0:T(8,128)(2,1)S(1)} %collective-permute-done.18), channel_id=1, source_target_pairs={{0,16},{1,241},{2,18},{3,243},{4,20},{5,245},{6,22},{7,247},{8,24}... | collective-permute-start | bytes 540680 | tf_op jit(solution)/shard_map/ppermute | solution.py:118
  66.0 8.1 %collective-permute-start.11 = (bf16[704,128]{1,0:T(8,128)(2,1)S(1)}, bf16[704,128]{1,0:T(8,128)(2,1)S(1)}, u32[]{:S(2)}, u32[]{:S(2)}) collective-permute-start(bf16[704,128]{1,0:T(8,128)(2,1)S(1)} %collective-permute-done.10), channel_id=1, source_target_pairs={{0,16},{1,241},{2,18},{3,243},{4,20},{5,245},{6,22},{7,247},{8,24}... | collective-permute-start | bytes 540680 | tf_op jit(solution)/shard_map/ppermute | solution.py:117
  69.1 7.5 %collective-permute-start.3 = (bf16[704,128]{1,0:T(8,128)(2,1)S(1)}, bf16[704,128]{1,0:T(8,128)(2,1)S(1)}, u32[]{:S(2)}, u32[]{:S(2)}) collective-permute-start(bf16[704,128]{1,0:T(8,128)(2,1)S(1)} %collective-permute-done.2), channel_id=1, source_target_pairs={{0,16},{1,241},{2,18},{3,243},{4,20},{5,245},{6,22},{7,247},{8,24}... | collective-permute-start | bytes 540680 | tf_op jit(solution)/shard_map/ppermute | solution.py:116
  71.1 7.5 %collective-permute-start.20 = (bf16[704,128]{1,0:T(8,128)(2,1)S(1)}, bf16[704,128]{1,0:T(8,128)(2,1)S(1)}, u32[]{:S(2)}, u32[]{:S(2)}) collective-permute-start(bf16[704,128]{1,0:T(8,128)(2,1)S(1)} %collective-permute-done.19), channel_id=1, source_target_pairs={{0,16},{1,241},{2,18},{3,243},{4,20},{5,245},{6,22},{7,247},{8,24}... | collective-permute-start | bytes 540680 | tf_op jit(solution)/shard_map/ppermute | solution.py:118
  74.0 7.5 %collective-permute-start.12 = (bf16[704,128]{1,0:T(8,128)(2,1)S(1)}, bf16[704,128]{1,0:T(8,128)(2,1)S(1)}, u32[]{:S(2)}, u32[]{:S(2)}) collective-permute-start(bf16[704,128]{1,0:T(8,128)(2,1)S(1)} %collective-permute-done.11), channel_id=1, source_target_pairs={{0,16},{1,241},{2,18},{3,243},{4,20},{5,245},{6,22},{7,247},{8,24}... | collective-permute-start | bytes 540680 | tf_op jit(solution)/shard_map/ppermute | solution.py:117
  76.6 7.5 %collective-permute-start.4 = (bf16[704,128]{1,0:T(8,128)(2,1)S(1)}, bf16[704,128]{1,0:T(8,128)(2,1)S(1)}, u32[]{:S(2)}, u32[]{:S(2)}) collective-permute-start(bf16[704,128]{1,0:T(8,128)(2,1)S(1)} %collective-permute-done.3), channel_id=1, source_target_pairs={{0,16},{1,241},{2,18},{3,243},{4,20},{5,245},{6,22},{7,247},{8,24}... | collective-permute-start | bytes 540680 | tf_op jit(solution)/shard_map/ppermute | solution.py:116
  78.5 7.5 %collective-permute-start.21 = (bf16[704,128]{1,0:T(8,128)(2,1)S(1)}, bf16[704,128]{1,0:T(8,128)(2,1)S(1)}, u32[]{:S(2)}, u32[]{:S(2)}) collective-permute-start(bf16[704,128]{1,0:T(8,128)(2,1)S(1)} %collective-permute-done.20), channel_id=1, source_target_pairs={{0,16},{1,241},{2,18},{3,243},{4,20},{5,245},{6,22},{7,247},{8,24}... | collective-permute-start | bytes 540680 | tf_op jit(solution)/shard_map/ppermute | solution.py:118
  81.5 6.9 %collective-permute-start.13 = (bf16[704,128]{1,0:T(8,128)(2,1)S(1)}, bf16[704,128]{1,0:T(8,128)(2,1)S(1)}, u32[]{:S(2)}, u32[]{:S(2)}) collective-permute-start(bf16[704,128]{1,0:T(8,128)(2,1)S(1)} %collective-permute-done.12), channel_id=1, source_target_pairs={{0,16},{1,241},{2,18},{3,243},{4,20},{5,245},{6,22},{7,247},{8,24}... | collective-permute-start | bytes 540680 | tf_op jit(solution)/shard_map/ppermute | solution.py:117
  84.0 39.9 %collective-permute-start.5 = (bf16[704,128]{1,0:T(8,128)(2,1)S(1)}, bf16[704,128]{1,0:T(8,128)(2,1)S(1)}, u32[]{:S(2)}, u32[]{:S(2)}) collective-permute-start(bf16[704,128]{1,0:T(8,128)(2,1)S(1)} %collective-permute-done.4), channel_id=1, source_target_pairs={{0,16},{1,241},{2,18},{3,243},{4,20},{5,245},{6,22},{7,247},{8,24}... | collective-permute-start | bytes 540680 | tf_op jit(solution)/shard_map/ppermute | solution.py:116
  86.0 39.9 %collective-permute-start.22 = (bf16[704,128]{1,0:T(8,128)(2,1)S(1)}, bf16[704,128]{1,0:T(8,128)(2,1)S(1)}, u32[]{:S(2)}, u32[]{:S(2)}) collective-permute-start(bf16[704,128]{1,0:T(8,128)(2,1)S(1)} %collective-permute-done.21), channel_id=1, source_target_pairs={{0,16},{1,241},{2,18},{3,243},{4,20},{5,245},{6,22},{7,247},{8,24}... | collective-permute-start | bytes 540680 | tf_op jit(solution)/shard_map/ppermute | solution.py:118
  88.4 6.3 %collective-permute-start.14 = (bf16[704,128]{1,0:T(8,128)(2,1)S(1)}, bf16[704,128]{1,0:T(8,128)(2,1)S(1)}, u32[]{:S(2)}, u32[]{:S(2)}) collective-permute-start(bf16[704,128]{1,0:T(8,128)(2,1)S(1)} %collective-permute-done.13), channel_id=1, source_target_pairs={{0,16},{1,241},{2,18},{3,243},{4,20},{5,245},{6,22},{7,247},{8,24}... | collective-permute-start | bytes 540680 | tf_op jit(solution)/shard_map/ppermute | solution.py:117
  94.7 11.4 %collective-permute-start.15 = (bf16[704,128]{1,0:T(8,128)(2,1)S(1)}, bf16[704,128]{1,0:T(8,128)(2,1)S(1)}, u32[]{:S(2)}, u32[]{:S(2)}) collective-permute-start(bf16[704,128]{1,0:T(8,128)(2,1)S(1)} %collective-permute-done.14), channel_id=1, source_target_pairs={{0,16},{1,241},{2,18},{3,243},{4,20},{5,245},{6,22},{7,247},{8,24}... | collective-permute-start | bytes 540680 | tf_op jit(solution)/shard_map/ppermute | solution.py:117
  106.6 30.2 %collective-permute-start.16 = (bf16[704,512]{1,0:T(8,128)(2,1)S(1)}, bf16[704,512]{1,0:T(8,128)(2,1)S(1)}, u32[]{:S(2)}, u32[]{:S(2)}) collective-permute-start(bf16[704,512]{1,0:T(8,128)(2,1)S(1)} %fusion.1), channel_id=1, source_target_pairs={{0,1},{1,0},{2,3},{3,2},{4,5},{5,4},{6,7},{7,6},{8,9},{9,8},{10,11... | collective-permute-start | bytes 2162696 | tf_op jit(solution)/shard_map/ppermute | solution.py:124
  123.9 6.6 %collective-permute-start.6 = (bf16[704,128]{1,0:T(8,128)(2,1)S(1)}, bf16[704,128]{1,0:T(8,128)(2,1)S(1)}, u32[]{:S(2)}, u32[]{:S(2)}) collective-permute-start(bf16[704,128]{1,0:T(8,128)(2,1)S(1)} %collective-permute-done.5), channel_id=1, source_target_pairs={{0,16},{1,241},{2,18},{3,243},{4,20},{5,245},{6,22},{7,247},{8,24}... | collective-permute-start | bytes 540680 | tf_op jit(solution)/shard_map/ppermute | solution.py:116
  125.9 18.1 %collective-permute-start.23 = (bf16[704,128]{1,0:T(8,128)(2,1)S(1)}, bf16[704,128]{1,0:T(8,128)(2,1)S(1)}, u32[]{:S(2)}, u32[]{:S(2)}) collective-permute-start(bf16[704,128]{1,0:T(8,128)(2,1)S(1)} %collective-permute-done.22), channel_id=1, source_target_pairs={{0,16},{1,241},{2,18},{3,243},{4,20},{5,245},{6,22},{7,247},{8,24}... | collective-permute-start | bytes 540680 | tf_op jit(solution)/shard_map/ppermute | solution.py:118
  130.5 6.3 %collective-permute-start.7 = (bf16[704,128]{1,0:T(8,128)(2,1)S(1)}, bf16[704,128]{1,0:T(8,128)(2,1)S(1)}, u32[]{:S(2)}, u32[]{:S(2)}) collective-permute-start(bf16[704,128]{1,0:T(8,128)(2,1)S(1)} %collective-permute-done.6), channel_id=1, source_target_pairs={{0,16},{1,241},{2,18},{3,243},{4,20},{5,245},{6,22},{7,247},{8,24}... | collective-permute-start | bytes 540680 | tf_op jit(solution)/shard_map/ppermute | solution.py:116
  133.8 3.4 %copy-start.3 = (f32[352]{0:T(512)S(1)}, f32[352]{0:T(512)}, u32[]{:S(2)}) copy-start(f32[352]{0:T(512)} %param.14) | copy-start | bytes 4228
  133.8 3.4 %copy-start.4 = (f32[352]{0:T(512)S(1)}, f32[352]{0:T(512)}, u32[]{:S(2)}) copy-start(f32[352]{0:T(512)} %param.12) | copy-start | bytes 4228
  137.5 13.1 %collective-permute-start.17 = (bf16[352,512]{1,0:T(8,128)(2,1)S(1)}, bf16[352,512]{1,0:T(8,128)(2,1)S(1)}, u32[]{:S(2)}, u32[]{:S(2)}) collective-permute-start(bf16[352,512]{1,0:T(8,128)(2,1)S(1)} %fusion.3), channel_id=1, source_target_pairs={{0,1},{1,0},{2,3},{3,2},{4,5},{5,4},{6,7},{7,6},{8,9},{9,8},{10,11... | collective-permute-start | bytes 1081352 | tf_op jit(solution)/shard_map/ppermute | solution.py:129
  144.0 6.6 %collective-permute-start.24 = (bf16[704,128]{1,0:T(8,128)(2,1)S(1)}, bf16[704,128]{1,0:T(8,128)(2,1)S(1)}, u32[]{:S(2)}, u32[]{:S(2)}) collective-permute-start(bf16[704,128]{1,0:T(8,128)(2,1)S(1)} %collective-permute-done.23), channel_id=1, source_target_pairs={{0,16},{1,241},{2,18},{3,243},{4,20},{5,245},{6,22},{7,247},{8,24}... | collective-permute-start | bytes 540680 | tf_op jit(solution)/shard_map/ppermute | solution.py:118
  212.2 9.3 %copy-start.1 = (bf16[8,64,1024]{2,1,0:T(8,128)(2,1)}, bf16[8,64,1024]{2,1,0:T(8,128)(2,1)S(1)}, u32[]{:S(2)}) copy-start(bf16[8,64,1024]{2,1,0:T(8,128)(2,1)S(1)} %all_to_all.11) | copy-start | bytes 3145732
  212.2 9.3 %collective-permute-start.25 = (bf16[512,1024]{1,0:T(8,128)(2,1)S(1)}, bf16[512,1024]{1,0:T(8,128)(2,1)S(1)}, u32[]{:S(2)}, u32[]{:S(2)}) collective-permute-start(bf16[512,1024]{1,0:T(8,128)(2,1)S(1)} %bitcast.25), channel_id=1, source_target_pairs={{0,1},{1,0},{2,3},{3,2},{4,5},{5,4},{6,7},{7,6},{8,9},{9,8},{10,11... | collective-permute-start | bytes 3145736 | tf_op jit(solution)/shard_map/ppermute | solution.py:145
  221.5 1.0 copy-start.2

commit v2 on v1

v2 whole, which is shorter than its diff:
```python
import jax
import jax.numpy as jnp
from jax import lax
from jax.experimental import pallas as pl
from jax.experimental.pallas import tpu as pltpu
from jax.sharding import PartitionSpec as P


EPS = 1e-06
LANES = 128
CORES = 2
ROWS = 64
CHUNKS = 1
FINISH_VMEM = 12 << 20
CHAINS = ("own", "other", "down")


def flat(z, t, n_fs, n_tp):
    return (z % n_fs) * n_tp + t


def patterns(n_fs, n_tp):
    enter, own, ring = ([], [], [])
    for z in range(n_fs):
        for t in range(n_tp):
            here = flat(z, t, n_fs, n_tp)
            if t % CORES == 0:
                enter.append((here, flat(z, t + 1, n_fs, n_tp)))
                own.append((here, flat(z + 1, t, n_fs, n_tp)))
                ring.append((here, flat(z + 1, t, n_fs, n_tp)))
            else:
                enter.append((here, flat(z + 1, t - 1, n_fs, n_tp)))
                ring.append((here, flat(z - 1, t, n_fs, n_tp)))
    return enter, own, ring


def finish_kernel(n_fs, place, mine, other, scale, gain, *outs):
    out = outs[-1]
    z, core = (place[0], place[1])
    slots = mine.shape[1] // LANES
    at_rows = pl.ds(pl.multiple_of(pl.program_id(0) * ROWS, ROWS), ROWS)
    total = None
    branches = []
    for held, which in ((mine, core), (other, 1 - core)):
        for k in range(slots):
            slab = lax.rem(jnp.where(which == 0, z - 1 - k, z + k) + n_fs, n_fs)
            branch = held[at_rows, k * LANES : (k + 1) * LANES].astype(jnp.float32)
            branch = branch * scale[pl.ds(slab, 1), :]
            squares = branch * branch
            total = squares if total is None else total + squares
            branches.append((slab, branch))
    width = LANES * len(branches)
    norm = lax.rsqrt(jnp.sum(total, axis=-1, keepdims=True) / width + EPS)
    for slab, branch in branches:
        at = pl.multiple_of(slab * LANES, LANES)
        out[:, pl.ds(at, LANES)] = (branch * norm * gain[pl.ds(slab, 1), :]).astype(out.dtype)


def finish(place, mine, other, scale, gain, n_fs, chunk, n_rows, done):
    rows, half = mine.shape
    first = chunk * rows // ROWS
    whole = pl.BlockSpec(memory_space=pltpu.VMEM)
    earlier = [] if done is None else [done]
    return pl.pallas_call(
        lambda *refs: finish_kernel(n_fs, *refs),
        grid_spec=pltpu.PrefetchScalarGridSpec(
            num_scalar_prefetch=1,
            grid=(rows // ROWS,),
            in_specs=[whole] * 4 + [pl.BlockSpec(memory_space=pl.ANY)] * len(earlier),
            out_specs=pl.BlockSpec((ROWS, 2 * half), lambda i, place: (first + i, 0)),
        ),
        out_shape=jax.ShapeDtypeStruct((n_rows, 2 * half), jnp.bfloat16),
        input_output_aliases={5: 0} if earlier else {},
        compiler_params=pltpu.CompilerParams(vmem_limit_bytes=FINISH_VMEM),
    )(place, mine, other, scale, gain, *earlier)


def body(
    tokens,
    pre_gain,
    gate_weight,
    gate_scale,
    up_weight,
    up_scale,
    down_weight,
    down_scale,
    post_gain,
):
    n_fs, n_tp = (lax.axis_size("fs"), lax.axis_size("tp"))
    both = ("fs", "tp")
    z, t = (lax.axis_index("fs"), lax.axis_index("tp"))
    core = t % CORES
    enter, own_first, ring = patterns(n_fs, n_tp)
    partner = [(i, i ^ 1) for i in range(n_tp)]
    chips = [[x * CORES + c for x in range(n_tp // CORES)] for c in range(CORES)]
    n_chips = n_tp // CORES
    low = jnp.bfloat16
    units = gate_weight.shape[1]

    packed = jnp.concatenate(
        [
            (gate_weight * gate_scale).astype(low).T,
            (up_weight * up_scale).astype(low).T,
            down_weight.astype(low),
        ],
        axis=0,
    )
    other0 = lax.ppermute(packed, both, enter)
    shifted = lax.ppermute(packed, both, own_first)
    own0 = jnp.where(core == 0, shifted, packed)

    rows = tokens.astype(jnp.float32)
    inverse = lax.rsqrt(jnp.mean(rows * rows, axis=-1, keepdims=True) + EPS)

    def normed_slab(k):
        slab = jnp.where(core == 0, z - 1 - k, z + k) % n_fs
        part = lax.dynamic_slice_in_dim(tokens, slab * LANES, LANES, axis=1).astype(jnp.float32)
        return (part * inverse * lax.dynamic_slice_in_dim(pre_gain, slab * LANES, LANES)).astype(low)

    def product(weights, k_normed):
        return lax.dot_general(
            weights, k_normed, (((1,), (1,)), ((), ())), preferred_element_type=jnp.float32
        )

    held = {
        "own": own0[: 2 * units],
        "other": other0[: 2 * units],
        "down": jnp.concatenate([own0[2 * units :], other0[2 * units :]], axis=0),
    }
    downs = [held["down"]]
    slab = normed_slab(0)
    sum_own, sum_other = (product(held["own"], slab), product(held["other"], slab))
    for k in range(1, n_fs // 2):
        for chain in CHAINS:
            held[chain] = lax.ppermute(held[chain], both, ring)
        downs.append(held["down"])
        slab = normed_slab(k)
        sum_own = sum_own + product(held["own"], slab)
        sum_other = sum_other + product(held["other"], slab)

    sums = jnp.concatenate([sum_own, sum_other], axis=0).astype(low)
    arrived = lax.ppermute(sums, "tp", partner)

    def gated(sums, more):
        sums = sums + more.astype(jnp.float32)
        return (jax.nn.silu(sums[:units]) * sums[units:]).astype(low)

    hidden = jnp.concatenate(
        [gated(sum_own, arrived[2 * units :]), gated(sum_other, arrived[: 2 * units])], axis=0
    )
    columns = jnp.concatenate(downs, axis=1)

    n_rows = tokens.shape[0]
    lines = n_rows // CHUNKS
    scale, gain = (down_scale.reshape(-1, LANES), post_gain.reshape(-1, LANES))
    place = jnp.stack([z, core]).astype(jnp.int32)

    def over_chips(array):
        return lax.all_to_all(array, "tp", 0, 0, axis_index_groups=chips, tiled=True)

    parts = []
    for c in range(CHUNKS):
        partial = lax.dot_general(
            hidden[:, c * lines : (c + 1) * lines],
            columns,
            (((0,), (0,)), ((), ())),
            preferred_element_type=jnp.float32,
        ).astype(low)
        parts.append(over_chips(partial.reshape(n_chips, lines // n_chips, -1)))
    mines = []
    for part in parts:
        summed = jnp.sum(part.astype(jnp.float32), axis=0).astype(low)
        mines.append(over_chips(jnp.broadcast_to(summed, part.shape)).reshape(lines, -1))
    out = None
    for c, mine in enumerate(mines):
        other = lax.ppermute(mine, "tp", partner)
        out = finish(place, mine, other, scale, gain, n_fs, c, n_rows, out)
    return out


def solution(mesh):
    in_specs = (
        P(("grp", "fs"), None),
        P(),
        P("fs", "tp"),
        P("tp"),
        P("fs", "tp"),
        P("tp"),
        P("tp", "fs"),
        P(),
        P(),
    )
    out_specs = P(("grp", "fs"), None)

    return jax.shard_map(body, mesh=mesh, in_specs=in_specs, out_specs=out_specs, check_vma=False)
```

time: 229 us -> 235 us (1.026)
  starting transfers between devices: 129 us -> 145 us
  blocking collectives: 60.3 us -> 48 us
  waiting for transfers between devices: 17.4 us -> 21.2 us
    all_to_all x2, blocking collectives: 60.3 us -> 48 us  [over_chips(): lax.all_to_all(array, 'tp', 0, 0, axis_index_groups=chips, tiled=True)]
    ppermute x23 -> x22, starting transfers between devices: 116 us -> 127 us  [the longest x21 112 us: body(): held[chain] = lax.ppermute(held[chain], both, ring)]
    ppermute x1, starting transfers between devices: 7.01 us -> 12.3 us  [body(): other = lax.ppermute(mine, 'tp', partner)]
    ppermute x23 -> x22, waiting for transfers between devices: 15.7 us -> 19 us  [the longest x21 19 us: body(): held[chain] = lax.ppermute(held[chain], both, ring)]
  transfers between devices with their start and end apart: 26 -> 25, of which waited for: 7 -> 10; matrix products, arithmetic and copies ran while one was open for 5% -> 4% of each run, Pallas kernels for 0% -> 0%
where the time goes in v2:
time: 235 us; the launch traced here: 234 us
  starting transfers between devices  145 us (62%)
  blocking collectives  48 us (20%)
  waiting for transfers between devices  21.2 us (9%)
  matrix products  8.31 us (4%)
  other arithmetic  5.64 us (2%)
  Pallas kernels  4.51 us (2%)
    ppermute x21, starting transfers between devices, body(): held[chain] = lax.ppermute(held[chain], both, ring)  112 us
    all_to_all x2, blocking collectives, over_chips(): lax.all_to_all(array, 'tp', 0, 0, axis_index_groups=chips, tiled=True)  48 us
    ppermute x21, waiting for transfers between devices, body(): held[chain] = lax.ppermute(held[chain], both, ring)  19 us
    ppermute x1, starting transfers between devices, body(): arrived = lax.ppermute(sums, 'tp', partner)  14.6 us
    ppermute x1, starting transfers between devices, body(): other = lax.ppermute(mine, 'tp', partner)  12.3 us
    dot_general x16, matrix products, product(): lax.dot_general(weights, k_normed, (((1,), (1,)), ((), ())), preferred_el...  7.31 us
    ppermute x1, starting transfers between devices, body(): other0 = lax.ppermute(packed, both, enter)  5.17 us
  transfers between devices with their start and end apart: 25, of which 10 were waited for; matrix products, arithmetic and copies ran while one was open for 4% of the time, Pallas kernels for 0%

profile of v2, /device:TPU:65, one launch (start us, length us, event | category | flops | bytes accessed | tf_op | source)
XLA Modules:
  0.0 234.0 jit_solution(12718878142073233907)
XLA Ops:
  0.0 0.9 convert_element_type.80
  0.9 1.2 fusion.5
  2.2 5.2 %collective-permute-start.8 = (bf16[1056,128]{1,0:T(8,128)(2,1)S(1)}, bf16[1056,128]{1,0:T(8,128)(2,1)S(1)}, u32[]{:S(2)}, u32[]{:S(2)}) collective-permute-start(bf16[1056,128]{1,0:T(8,128)(2,1)S(1)} %pad_maximum_fusion.1), channel_id=1, source_target_pairs={{0,1},{1,16},{2,3},{3,18},{4,5},{5,20},{6,7},{7,22},{8,9},{9,24},{... | collective-permute-start | bytes 811016 | tf_op jit(solution)/shard_map/ppermute | solution.py:108
  7.3 0.7 collective-permute-start
  8.0 2.1 multiply_reduce_fusion
  10.4 40.9 %collective-permute-start.1 = (bf16[704,128]{1,0:T(8,128)(2,1)S(1)}, bf16[704,128]{1,0:T(8,128)(2,1)S(1)}, u32[]{:S(2)}, u32[]{:S(2)}) collective-permute-start(bf16[704,128]{1,0:T(8,128)(2,1)S(1)} %slice.40), channel_id=1, source_target_pairs={{0,16},{1,241},{2,18},{3,243},{4,20},{5,245},{6,22},{7,247},{8,24}... | collective-permute-start | bytes 540680 | tf_op jit(solution)/shard_map/ppermute | solution.py:135
  51.5 2.5 %collective-permute-start.9 = (bf16[704,128]{1,0:T(8,128)(2,1)S(1)}, bf16[704,128]{1,0:T(8,128)(2,1)S(1)}, u32[]{:S(2)}, u32[]{:S(2)}) collective-permute-start(bf16[704,128]{1,0:T(8,128)(2,1)S(1)} %slice.41), channel_id=1, source_target_pairs={{0,16},{1,241},{2,18},{3,243},{4,20},{5,245},{6,22},{7,247},{8,24}... | collective-permute-start | bytes 540680 | tf_op jit(solution)/shard_map/ppermute | solution.py:135
  54.2 2.0 collective-permute-start.17
  57.1 0.8 collective-permute-done.9
  58.3 3.7 %collective-permute-start.10 = (bf16[704,128]{1,0:T(8,128)(2,1)S(1)}, bf16[704,128]{1,0:T(8,128)(2,1)S(1)}, u32[]{:S(2)}, u32[]{:S(2)}) collective-permute-start(bf16[704,128]{1,0:T(8,128)(2,1)S(1)} %collective-permute-done.9), channel_id=1, source_target_pairs={{0,16},{1,241},{2,18},{3,243},{4,20},{5,245},{6,22},{7,247},{8,24}... | collective-permute-start | bytes 540680 | tf_op jit(solution)/shard_map/ppermute | solution.py:135
  62.0 2.0 collective-permute-start.2
  64.8 4.6 %collective-permute-start.11 = (bf16[704,128]{1,0:T(8,128)(2,1)S(1)}, bf16[704,128]{1,0:T(8,128)(2,1)S(1)}, u32[]{:S(2)}, u32[]{:S(2)}) collective-permute-start(bf16[704,128]{1,0:T(8,128)(2,1)S(1)} %collective-permute-done.10), channel_id=1, source_target_pairs={{0,16},{1,241},{2,18},{3,243},{4,20},{5,245},{6,22},{7,247},{8,24}... | collective-permute-start | bytes 540680 | tf_op jit(solution)/shard_map/ppermute | solution.py:135
  69.5 2.0 collective-permute-start.3
  72.4 4.6 %collective-permute-start.12 = (bf16[704,128]{1,0:T(8,128)(2,1)S(1)}, bf16[704,128]{1,0:T(8,128)(2,1)S(1)}, u32[]{:S(2)}, u32[]{:S(2)}) collective-permute-start(bf16[704,128]{1,0:T(8,128)(2,1)S(1)} %collective-permute-done.11), channel_id=1, source_target_pairs={{0,16},{1,241},{2,18},{3,243},{4,20},{5,245},{6,22},{7,247},{8,24}... | collective-permute-start | bytes 540680 | tf_op jit(solution)/shard_map/ppermute | solution.py:135
  77.0 2.0 collective-permute-start.4
  78.9 0.5 convolution_add_fusion.4
  79.4 0.5 convolution_add_fusion.11
  79.9 4.5 %collective-permute-start.13 = (bf16[704,128]{1,0:T(8,128)(2,1)S(1)}, bf16[704,128]{1,0:T(8,128)(2,1)S(1)}, u32[]{:S(2)}, u32[]{:S(2)}) collective-permute-start(bf16[704,128]{1,0:T(8,128)(2,1)S(1)} %collective-permute-done.12), channel_id=1, source_target_pairs={{0,16},{1,241},{2,18},{3,243},{4,20},{5,245},{6,22},{7,247},{8,24}... | collective-permute-start | bytes 540680 | tf_op jit(solution)/shard_map/ppermute | solution.py:135
  84.4 2.0 collective-permute-start.5
  86.4 0.5 convolution_add_fusion.3
  87.3 4.5 %collective-permute-start.14 = (bf16[704,128]{1,0:T(8,128)(2,1)S(1)}, bf16[704,128]{1,0:T(8,128)(2,1)S(1)}, u32[]{:S(2)}, u32[]{:S(2)}) collective-permute-start(bf16[704,128]{1,0:T(8,128)(2,1)S(1)} %collective-permute-done.13), channel_id=1, source_target_pairs={{0,16},{1,241},{2,18},{3,243},{4,20},{5,245},{6,22},{7,247},{8,24}... | collective-permute-start | bytes 540680 | tf_op jit(solution)/shard_map/ppermute | solution.py:135
  91.9 2.0 collective-permute-start.6
  93.9 0.5 convolution_add_fusion.2
  94.8 4.5 %collective-permute-start.15 = (bf16[704,128]{1,0:T(8,128)(2,1)S(1)}, bf16[704,128]{1,0:T(8,128)(2,1)S(1)}, u32[]{:S(2)}, u32[]{:S(2)}) collective-permute-start(bf16[704,128]{1,0:T(8,128)(2,1)S(1)} %collective-permute-done.14), channel_id=1, source_target_pairs={{0,16},{1,241},{2,18},{3,243},{4,20},{5,245},{6,22},{7,247},{8,24}... | collective-permute-start | bytes 540680 | tf_op jit(solution)/shard_map/ppermute | solution.py:135
  99.4 2.0 collective-permute-start.7
  101.3 0.5 convolution_add_fusion.1
  102.3 0.5 fusion.29
  102.7 3.2 %collective-permute-done.7 = bf16[704,128]{1,0:T(8,128)(2,1)S(1)} collective-permute-done((bf16[704,128]{1,0:T(8,128)(2,1)S(1)}, bf16[704,128]{1,0:T(8,128)(2,1)S(1)}, u32[]{:S(2)}, u32[]{:S(2)}) %collective-permute-start.7) | collective-permute-done | bytes 180256 | tf_op jit(solution)/shard_map/ppermute | solution.py:135
  106.5 14.6 %collective-permute-start.16 = (bf16[1408,512]{1,0:T(8,128)(2,1)S(1)}, bf16[1408,512]{1,0:T(8,128)(2,1)S(1)}, u32[]{:S(2)}, u32[]{:S(2)}) collective-permute-start(bf16[1408,512]{1,0:T(8,128)(2,1)S(1)} %pad_maximum_fusion), channel_id=1, source_target_pairs={{0,1},{1,0},{2,3},{3,2},{4,5},{5,4},{6,7},{7,6},{8,9},{9,8},{10,11... | collective-permute-start | bytes 4325384 | tf_op jit(solution)/shard_map/ppermute | solution.py:142
  121.2 3.7 %collective-permute-start.18 = (bf16[704,128]{1,0:T(8,128)(2,1)S(1)}, bf16[704,128]{1,0:T(8,128)(2,1)S(1)}, u32[]{:S(2)}, u32[]{:S(2)}) collective-permute-start(bf16[704,128]{1,0:T(8,128)(2,1)S(1)} %collective-permute-done.17), channel_id=1, source_target_pairs={{0,16},{1,241},{2,18},{3,243},{4,20},{5,245},{6,22},{7,247},{8,24}... | collective-permute-start | bytes 540680 | tf_op jit(solution)/shard_map/ppermute | solution.py:135
  124.8 2.9 %collective-permute-done.18 = bf16[704,128]{1,0:T(8,128)(2,1)S(1)} collective-permute-done((bf16[704,128]{1,0:T(8,128)(2,1)S(1)}, bf16[704,128]{1,0:T(8,128)(2,1)S(1)}, u32[]{:S(2)}, u32[]{:S(2)}) %collective-permute-start.18) | collective-permute-done | bytes 180256 | tf_op jit(solution)/shard_map/ppermute | solution.py:135
  127.7 4.6 %collective-permute-start.19 = (bf16[704,128]{1,0:T(8,128)(2,1)S(1)}, bf16[704,128]{1,0:T(8,128)(2,1)S(1)}, u32[]{:S(2)}, u32[]{:S(2)}) collective-permute-start(bf16[704,128]{1,0:T(8,128)(2,1)S(1)} %collective-permute-done.18), channel_id=1, source_target_pairs={{0,16},{1,241},{2,18},{3,243},{4,20},{5,245},{6,22},{7,247},{8,24}... | collective-permute-start | bytes 540680 | tf_op jit(solution)/shard_map/ppermute | solution.py:135
  132.3 2.4 %collective-permute-done.19 = bf16[704,128]{1,0:T(8,128)(2,1)S(1)} collective-permute-done((bf16[704,128]{1,0:T(8,128)(2,1)S(1)}, bf16[704,128]{1,0:T(8,128)(2,1)S(1)}, u32[]{:S(2)}, u32[]{:S(2)}) %collective-permute-start.19) | collective-permute-done | bytes 180256 | tf_op jit(solution)/shard_map/ppermute | solution.py:135
  134.7 5.0 %collective-permute-start.20 = (bf16[704,128]{1,0:T(8,128)(2,1)S(1)}, bf16[704,128]{1,0:T(8,128)(2,1)S(1)}, u32[]{:S(2)}, u32[]{:S(2)}) collective-permute-start(bf16[704,128]{1,0:T(8,128)(2,1)S(1)} %collective-permute-done.19), channel_id=1, source_target_pairs={{0,16},{1,241},{2,18},{3,243},{4,20},{5,245},{6,22},{7,247},{8,24}... | collective-permute-start | bytes 540680 | tf_op jit(solution)/shard_map/ppermute | solution.py:135
  139.8 2.4 %collective-permute-done.20 = bf16[704,128]{1,0:T(8,128)(2,1)S(1)} collective-permute-done((bf16[704,128]{1,0:T(8,128)(2,1)S(1)}, bf16[704,128]{1,0:T(8,128)(2,1)S(1)}, u32[]{:S(2)}, u32[]{:S(2)}) %collective-permute-start.20) | collective-permute-done | bytes 180256 | tf_op jit(solution)/shard_map/ppermute | solution.py:135
  142.2 5.0 %collective-permute-start.21 = (bf16[704,128]{1,0:T(8,128)(2,1)S(1)}, bf16[704,128]{1,0:T(8,128)(2,1)S(1)}, u32[]{:S(2)}, u32[]{:S(2)}) collective-permute-start(bf16[704,128]{1,0:T(8,128)(2,1)S(1)} %collective-permute-done.20), channel_id=1, source_target_pairs={{0,16},{1,241},{2,18},{3,243},{4,20},{5,245},{6,22},{7,247},{8,24}... | collective-permute-start | bytes 540680 | tf_op jit(solution)/shard_map/ppermute | solution.py:135
  147.4 2.3 collective-permute-done.21
  149.7 5.0 %collective-permute-start.22 = (bf16[704,128]{1,0:T(8,128)(2,1)S(1)}, bf16[704,128]{1,0:T(8,128)(2,1)S(1)}, u32[]{:S(2)}, u32[]{:S(2)}) collective-permute-start(bf16[704,128]{1,0:T(8,128)(2,1)S(1)} %collective-permute-done.21), channel_id=1, source_target_pairs={{0,16},{1,241},{2,18},{3,243},{4,20},{5,245},{6,22},{7,247},{8,24}... | collective-permute-start | bytes 540680 | tf_op jit(solution)/shard_map/ppermute | solution.py:135
  154.8 2.3 collective-permute-done.22
  157.1 5.0 %collective-permute-start.23 = (bf16[704,128]{1,0:T(8,128)(2,1)S(1)}, bf16[704,128]{1,0:T(8,128)(2,1)S(1)}, u32[]{:S(2)}, u32[]{:S(2)}) collective-permute-start(bf16[704,128]{1,0:T(8,128)(2,1)S(1)} %collective-permute-done.22), channel_id=1, source_target_pairs={{0,16},{1,241},{2,18},{3,243},{4,20},{5,245},{6,22},{7,247},{8,24}... | collective-permute-start | bytes 540680 | tf_op jit(solution)/shard_map/ppermute | solution.py:135
  162.3 2.3 collective-permute-done.23
  164.7 0.5 convert_add_fusion.1
  165.6 1.0 convolution_convert_fusion
  166.6 25.4 %all_to_all.10 = bf16[8,64,1024]{2,1,0:T(8,128)(2,1)S(1)} all-to-all(bf16[8,64,1024]{2,1,0:T(8,128)(2,1)S(1)} %bitcast.29), channel_id=1, replica_groups={{0,2,4,6,8,10,12,14},{1,3,5,7,9,11,13,15},{16,18,20,22,24,26,28,30},{17..., dimensions={0} | all-to-all | bytes 2097152 | tf_op jit(solution)/shard_map/all_to_all | solution.py:159
  192.3 22.6 %all_to_all.11 = bf16[8,64,1024]{2,1,0:T(8,128)(2,1)S(1)} all-to-all(bf16[8,64,1024]{2,1,0:T(8,128)(2,1)S(1)} %broadcast_in_dim.2), channel_id=1, replica_groups={{0,2,4,6,8,10,12,14},{1,3,5,7,9,11,13,15},{16,18,20,22,24,26,28,30},{17..., dimensions={0} | all-to-all | bytes 2097152 | tf_op jit(solution)/shard_map/all_to_all | solution.py:159
  215.0 12.3 %collective-permute-start.24 = (bf16[512,1024]{1,0:T(8,128)(2,1)S(1)}, bf16[512,1024]{1,0:T(8,128)(2,1)S(1)}, u32[]{:S(2)}, u32[]{:S(2)}) collective-permute-start(bf16[512,1024]{1,0:T(8,128)(2,1)S(1)} %bitcast.25), channel_id=1, source_target_pairs={{0,1},{1,0},{2,3},{3,2},{4,5},{5,4},{6,7},{7,6},{8,9},{9,8},{10,11... | collective-permute-start | bytes 3145736 | tf_op jit(solution)/shard_map/ppermute | solution.py:176
  227.3 2.2 collective-permute-done.24.refs_2_
  229.5 4.5 %shard_map.91 = bf16[512,2048]{1,0:T(8,128)(2,1)} custom-call(s32[2]{0:T(128)S(1)} %pad_add_fusion.refs_0_, bf16[512,1024]{1,0:T(8,128)(2,1)S(1)} %bitcast.26, bf16[512,1024]{1,0:T(8,128)(2,1)S(1)} %collective-permute-done.24.refs_2_, f32[16,128]{1,0:T(8,128)S(1)} %bitcast.27, f32[16,128]{1,0:T(8,128)S(1)} %bitcast.28), custom_call_target="tpu_custom_call" | custom-call | tf_op jit(solution)/shard_map/pallas_call | solution.py:64
  (56 shorter events, 6.6 us)
Async XLA Ops:
  2.2 49.2 %copy-start.3 = (f32[2048]{0:T(1024)S(1)}, f32[2048]{0:T(1024)}, u32[]{:S(2)}) copy-start(f32[2048]{0:T(1024)} %param.10) | copy-start | bytes 24580
  2.2 49.4 %collective-permute-start.8 = (bf16[1056,128]{1,0:T(8,128)(2,1)S(1)}, bf16[1056,128]{1,0:T(8,128)(2,1)S(1)}, u32[]{:S(2)}, u32[]{:S(2)}) collective-permute-start(bf16[1056,128]{1,0:T(8,128)(2,1)S(1)} %pad_maximum_fusion.1), channel_id=1, source_target_pairs={{0,1},{1,16},{2,3},{3,18},{4,5},{5,20},{6,7},{7,22},{8,9},{9,24},{... | collective-permute-start | bytes 811016 | tf_op jit(solution)/shard_map/ppermute | solution.py:108
  7.3 3.0 %collective-permute-start = (bf16[1056,128]{1,0:T(8,128)(2,1)S(1)}, bf16[1056,128]{1,0:T(8,128)(2,1)S(1)}, u32[]{:S(2)}, u32[]{:S(2)}) collective-permute-start(bf16[1056,128]{1,0:T(8,128)(2,1)S(1)} %pad_maximum_fusion.1), channel_id=1, source_target_pairs={{0,16},{2,18},{4,20},{6,22},{8,24},{10,26},{12,28},{14,30},{16,32}... | collective-permute-start | bytes 811016 | tf_op jit(solution)/shard_map/ppermute | solution.py:109
  10.1 46.0 %copy-start.2 = (bf16[512,2048]{1,0:T(8,128)(2,1)S(1)}, bf16[512,2048]{1,0:T(8,128)(2,1)}, u32[]{:S(2)}) copy-start(bf16[512,2048]{1,0:T(8,128)(2,1)} %param.9) | copy-start | bytes 6291460
  10.4 45.7 %collective-permute-start.1 = (bf16[704,128]{1,0:T(8,128)(2,1)S(1)}, bf16[704,128]{1,0:T(8,128)(2,1)S(1)}, u32[]{:S(2)}, u32[]{:S(2)}) collective-permute-start(bf16[704,128]{1,0:T(8,128)(2,1)S(1)} %slice.40), channel_id=1, source_target_pairs={{0,16},{1,241},{2,18},{3,243},{4,20},{5,245},{6,22},{7,247},{8,24}... | collective-permute-start | bytes 540680 | tf_op jit(solution)/shard_map/ppermute | solution.py:135
  51.5 6.3 %collective-permute-start.9 = (bf16[704,128]{1,0:T(8,128)(2,1)S(1)}, bf16[704,128]{1,0:T(8,128)(2,1)S(1)}, u32[]{:S(2)}, u32[]{:S(2)}) collective-permute-start(bf16[704,128]{1,0:T(8,128)(2,1)S(1)} %slice.41), channel_id=1, source_target_pairs={{0,16},{1,241},{2,18},{3,243},{4,20},{5,245},{6,22},{7,247},{8,24}... | collective-permute-start | bytes 540680 | tf_op jit(solution)/shard_map/ppermute | solution.py:135
  54.2 67.0 %collective-permute-start.17 = (bf16[704,128]{1,0:T(8,128)(2,1)S(1)}, bf16[704,128]{1,0:T(8,128)(2,1)S(1)}, u32[]{:S(2)}, u32[]{:S(2)}) collective-permute-start(bf16[704,128]{1,0:T(8,128)(2,1)S(1)} %get-tuple-element.7), channel_id=1, source_target_pairs={{0,16},{1,241},{2,18},{3,243},{4,20},{5,245},{6,22},{7,247},{8,24}... | collective-permute-start | bytes 540680 | tf_op jit(solution)/shard_map/ppermute | solution.py:135
  58.3 6.6 %collective-permute-start.10 = (bf16[704,128]{1,0:T(8,128)(2,1)S(1)}, bf16[704,128]{1,0:T(8,128)(2,1)S(1)}, u32[]{:S(2)}, u32[]{:S(2)}) collective-permute-start(bf16[704,128]{1,0:T(8,128)(2,1)S(1)} %collective-permute-done.9), channel_id=1, source_target_pairs={{0,16},{1,241},{2,18},{3,243},{4,20},{5,245},{6,22},{7,247},{8,24}... | collective-permute-start | bytes 540680 | tf_op jit(solution)/shard_map/ppermute | solution.py:135
  62.0 7.5 %collective-permute-start.2 = (bf16[704,128]{1,0:T(8,128)(2,1)S(1)}, bf16[704,128]{1,0:T(8,128)(2,1)S(1)}, u32[]{:S(2)}, u32[]{:S(2)}) collective-permute-start(bf16[704,128]{1,0:T(8,128)(2,1)S(1)} %collective-permute-done.1), channel_id=1, source_target_pairs={{0,16},{1,241},{2,18},{3,243},{4,20},{5,245},{6,22},{7,247},{8,24}... | collective-permute-start | bytes 540680 | tf_op jit(solution)/shard_map/ppermute | solution.py:135
  64.8 7.5 %collective-permute-start.11 = (bf16[704,128]{1,0:T(8,128)(2,1)S(1)}, bf16[704,128]{1,0:T(8,128)(2,1)S(1)}, u32[]{:S(2)}, u32[]{:S(2)}) collective-permute-start(bf16[704,128]{1,0:T(8,128)(2,1)S(1)} %collective-permute-done.10), channel_id=1, source_target_pairs={{0,16},{1,241},{2,18},{3,243},{4,20},{5,245},{6,22},{7,247},{8,24}... | collective-permute-start | bytes 540680 | tf_op jit(solution)/shard_map/ppermute | solution.py:135
  69.5 7.5 %collective-permute-start.3 = (bf16[704,128]{1,0:T(8,128)(2,1)S(1)}, bf16[704,128]{1,0:T(8,128)(2,1)S(1)}, u32[]{:S(2)}, u32[]{:S(2)}) collective-permute-start(bf16[704,128]{1,0:T(8,128)(2,1)S(1)} %collective-permute-done.2), channel_id=1, source_target_pairs={{0,16},{1,241},{2,18},{3,243},{4,20},{5,245},{6,22},{7,247},{8,24}... | collective-permute-start | bytes 540680 | tf_op jit(solution)/shard_map/ppermute | solution.py:135
  72.4 7.5 %collective-permute-start.12 = (bf16[704,128]{1,0:T(8,128)(2,1)S(1)}, bf16[704,128]{1,0:T(8,128)(2,1)S(1)}, u32[]{:S(2)}, u32[]{:S(2)}) collective-permute-start(bf16[704,128]{1,0:T(8,128)(2,1)S(1)} %collective-permute-done.11), channel_id=1, source_target_pairs={{0,16},{1,241},{2,18},{3,243},{4,20},{5,245},{6,22},{7,247},{8,24}... | collective-permute-start | bytes 540680 | tf_op jit(solution)/shard_map/ppermute | solution.py:135
  77.0 7.5 %collective-permute-start.4 = (bf16[704,128]{1,0:T(8,128)(2,1)S(1)}, bf16[704,128]{1,0:T(8,128)(2,1)S(1)}, u32[]{:S(2)}, u32[]{:S(2)}) collective-permute-start(bf16[704,128]{1,0:T(8,128)(2,1)S(1)} %collective-permute-done.3), channel_id=1, source_target_pairs={{0,16},{1,241},{2,18},{3,243},{4,20},{5,245},{6,22},{7,247},{8,24}... | collective-permute-start | bytes 540680 | tf_op jit(solution)/shard_map/ppermute | solution.py:135
  79.9 7.5 %collective-permute-start.13 = (bf16[704,128]{1,0:T(8,128)(2,1)S(1)}, bf16[704,128]{1,0:T(8,128)(2,1)S(1)}, u32[]{:S(2)}, u32[]{:S(2)}) collective-permute-start(bf16[704,128]{1,0:T(8,128)(2,1)S(1)} %collective-permute-done.12), channel_id=1, source_target_pairs={{0,16},{1,241},{2,18},{3,243},{4,20},{5,245},{6,22},{7,247},{8,24}... | collective-permute-start | bytes 540680 | tf_op jit(solution)/shard_map/ppermute | solution.py:135
  84.4 7.5 %collective-permute-start.5 = (bf16[704,128]{1,0:T(8,128)(2,1)S(1)}, bf16[704,128]{1,0:T(8,128)(2,1)S(1)}, u32[]{:S(2)}, u32[]{:S(2)}) collective-permute-start(bf16[704,128]{1,0:T(8,128)(2,1)S(1)} %collective-permute-done.4), channel_id=1, source_target_pairs={{0,16},{1,241},{2,18},{3,243},{4,20},{5,245},{6,22},{7,247},{8,24}... | collective-permute-start | bytes 540680 | tf_op jit(solution)/shard_map/ppermute | solution.py:135
  87.3 7.5 %collective-permute-start.14 = (bf16[704,128]{1,0:T(8,128)(2,1)S(1)}, bf16[704,128]{1,0:T(8,128)(2,1)S(1)}, u32[]{:S(2)}, u32[]{:S(2)}) collective-permute-start(bf16[704,128]{1,0:T(8,128)(2,1)S(1)} %collective-permute-done.13), channel_id=1, source_target_pairs={{0,16},{1,241},{2,18},{3,243},{4,20},{5,245},{6,22},{7,247},{8,24}... | collective-permute-start | bytes 540680 | tf_op jit(solution)/shard_map/ppermute | solution.py:135
  91.9 7.5 %collective-permute-start.6 = (bf16[704,128]{1,0:T(8,128)(2,1)S(1)}, bf16[704,128]{1,0:T(8,128)(2,1)S(1)}, u32[]{:S(2)}, u32[]{:S(2)}) collective-permute-start(bf16[704,128]{1,0:T(8,128)(2,1)S(1)} %collective-permute-done.5), channel_id=1, source_target_pairs={{0,16},{1,241},{2,18},{3,243},{4,20},{5,245},{6,22},{7,247},{8,24}... | collective-permute-start | bytes 540680 | tf_op jit(solution)/shard_map/ppermute | solution.py:135
  94.8 7.5 %collective-permute-start.15 = (bf16[704,128]{1,0:T(8,128)(2,1)S(1)}, bf16[704,128]{1,0:T(8,128)(2,1)S(1)}, u32[]{:S(2)}, u32[]{:S(2)}) collective-permute-start(bf16[704,128]{1,0:T(8,128)(2,1)S(1)} %collective-permute-done.14), channel_id=1, source_target_pairs={{0,16},{1,241},{2,18},{3,243},{4,20},{5,245},{6,22},{7,247},{8,24}... | collective-permute-start | bytes 540680 | tf_op jit(solution)/shard_map/ppermute | solution.py:135
  99.4 6.6 %collective-permute-start.7 = (bf16[704,128]{1,0:T(8,128)(2,1)S(1)}, bf16[704,128]{1,0:T(8,128)(2,1)S(1)}, u32[]{:S(2)}, u32[]{:S(2)}) collective-permute-start(bf16[704,128]{1,0:T(8,128)(2,1)S(1)} %collective-permute-done.6), channel_id=1, source_target_pairs={{0,16},{1,241},{2,18},{3,243},{4,20},{5,245},{6,22},{7,247},{8,24}... | collective-permute-start | bytes 540680 | tf_op jit(solution)/shard_map/ppermute | solution.py:135
  106.5 58.2 %collective-permute-start.16 = (bf16[1408,512]{1,0:T(8,128)(2,1)S(1)}, bf16[1408,512]{1,0:T(8,128)(2,1)S(1)}, u32[]{:S(2)}, u32[]{:S(2)}) collective-permute-start(bf16[1408,512]{1,0:T(8,128)(2,1)S(1)} %pad_maximum_fusion), channel_id=1, source_target_pairs={{0,1},{1,0},{2,3},{3,2},{4,5},{5,4},{6,7},{7,6},{8,9},{9,8},{10,11... | collective-permute-start | bytes 4325384 | tf_op jit(solution)/shard_map/ppermute | solution.py:142
  121.2 6.6 %collective-permute-start.18 = (bf16[704,128]{1,0:T(8,128)(2,1)S(1)}, bf16[704,128]{1,0:T(8,128)(2,1)S(1)}, u32[]{:S(2)}, u32[]{:S(2)}) collective-permute-start(bf16[704,128]{1,0:T(8,128)(2,1)S(1)} %collective-permute-done.17), channel_id=1, source_target_pairs={{0,16},{1,241},{2,18},{3,243},{4,20},{5,245},{6,22},{7,247},{8,24}... | collective-permute-start | bytes 540680 | tf_op jit(solution)/shard_map/ppermute | solution.py:135
  127.7 7.0 %collective-permute-start.19 = (bf16[704,128]{1,0:T(8,128)(2,1)S(1)}, bf16[704,128]{1,0:T(8,128)(2,1)S(1)}, u32[]{:S(2)}, u32[]{:S(2)}) collective-permute-start(bf16[704,128]{1,0:T(8,128)(2,1)S(1)} %collective-permute-done.18), channel_id=1, source_target_pairs={{0,16},{1,241},{2,18},{3,243},{4,20},{5,245},{6,22},{7,247},{8,24}... | collective-permute-start | bytes 540680 | tf_op jit(solution)/shard_map/ppermute | solution.py:135
  134.7 7.5 %collective-permute-start.20 = (bf16[704,128]{1,0:T(8,128)(2,1)S(1)}, bf16[704,128]{1,0:T(8,128)(2,1)S(1)}, u32[]{:S(2)}, u32[]{:S(2)}) collective-permute-start(bf16[704,128]{1,0:T(8,128)(2,1)S(1)} %collective-permute-done.19), channel_id=1, source_target_pairs={{0,16},{1,241},{2,18},{3,243},{4,20},{5,245},{6,22},{7,247},{8,24}... | collective-permute-start | bytes 540680 | tf_op jit(solution)/shard_map/ppermute | solution.py:135
  142.2 7.5 %collective-permute-start.21 = (bf16[704,128]{1,0:T(8,128)(2,1)S(1)}, bf16[704,128]{1,0:T(8,128)(2,1)S(1)}, u32[]{:S(2)}, u32[]{:S(2)}) collective-permute-start(bf16[704,128]{1,0:T(8,128)(2,1)S(1)} %collective-permute-done.20), channel_id=1, source_target_pairs={{0,16},{1,241},{2,18},{3,243},{4,20},{5,245},{6,22},{7,247},{8,24}... | collective-permute-start | bytes 540680 | tf_op jit(solution)/shard_map/ppermute | solution.py:135
  149.7 7.5 %collective-permute-start.22 = (bf16[704,128]{1,0:T(8,128)(2,1)S(1)}, bf16[704,128]{1,0:T(8,128)(2,1)S(1)}, u32[]{:S(2)}, u32[]{:S(2)}) collective-permute-start(bf16[704,128]{1,0:T(8,128)(2,1)S(1)} %collective-permute-done.21), channel_id=1, source_target_pairs={{0,16},{1,241},{2,18},{3,243},{4,20},{5,245},{6,22},{7,247},{8,24}... | collective-permute-start | bytes 540680 | tf_op jit(solution)/shard_map/ppermute | solution.py:135
  157.1 7.5 %collective-permute-start.23 = (bf16[704,128]{1,0:T(8,128)(2,1)S(1)}, bf16[704,128]{1,0:T(8,128)(2,1)S(1)}, u32[]{:S(2)}, u32[]{:S(2)}) collective-permute-start(bf16[704,128]{1,0:T(8,128)(2,1)S(1)} %collective-permute-done.22), channel_id=1, source_target_pairs={{0,16},{1,241},{2,18},{3,243},{4,20},{5,245},{6,22},{7,247},{8,24}... | collective-permute-start | bytes 540680 | tf_op jit(solution)/shard_map/ppermute | solution.py:135
  192.2 37.3 %copy-start = (f32[2048]{0:T(1024)S(1)}, f32[2048]{0:T(1024)}, u32[]{:S(2)}) copy-start(f32[2048]{0:T(1024)} %param.16) | copy-start | bytes 24580
  192.2 37.3 %copy-start.1 = (f32[2048]{0:T(1024)S(1)}, f32[2048]{0:T(1024)}, u32[]{:S(2)}) copy-start(f32[2048]{0:T(1024)} %param.17) | copy-start | bytes 24580
  215.0 14.5 %collective-permute-start.24 = (bf16[512,1024]{1,0:T(8,128)(2,1)S(1)}, bf16[512,1024]{1,0:T(8,128)(2,1)S(1)}, u32[]{:S(2)}, u32[]{:S(2)}) collective-permute-start(bf16[512,1024]{1,0:T(8,128)(2,1)S(1)} %bitcast.25), channel_id=1, source_target_pairs={{0,1},{1,0},{2,3},{3,2},{4,5},{5,4},{6,7},{7,6},{8,9},{9,8},{10,11... | collective-permute-start | bytes 3145736 | tf_op jit(solution)/shard_map/ppermute | solution.py:176

commit v3 on v2

--- a/solution.py
+++ b/solution.py
@@ -26,12 +26,16 @@
             here = flat(z, t, n_fs, n_tp)
             if t % CORES == 0:
                 enter.append((here, flat(z, t + 1, n_fs, n_tp)))
-                own.append((here, flat(z + 1, t, n_fs, n_tp)))
+                own.append((here, flat(z - 1, t, n_fs, n_tp)))
+                ring.append((here, flat(z - 1, t, n_fs, n_tp)))
+            else:
+                enter.append((here, flat(z - 1, t - 1, n_fs, n_tp)))
                 ring.append((here, flat(z + 1, t, n_fs, n_tp)))
-            else:
-                enter.append((here, flat(z + 1, t - 1, n_fs, n_tp)))
-                ring.append((here, flat(z - 1, t, n_fs, n_tp)))
     return enter, own, ring
+
+
+def slab_of(slot, core, z, n_fs):
+    return lax.rem(jnp.where(core == 0, z + 1 + slot, z - slot + n_fs), n_fs)
 
 
 def finish_kernel(n_fs, place, mine, other, scale, gain, *outs):
@@ -43,7 +47,7 @@
     branches = []
     for held, which in ((mine, core), (other, 1 - core)):
         for k in range(slots):
-            slab = lax.rem(jnp.where(which == 0, z - 1 - k, z + k) + n_fs, n_fs)
+            slab = slab_of(k, which, z, n_fs)
             branch = held[at_rows, k * LANES : (k + 1) * LANES].astype(jnp.float32)
             branch = branch * scale[pl.ds(slab, 1), :]
             squares = branch * branch
@@ -113,7 +117,7 @@
     inverse = lax.rsqrt(jnp.mean(rows * rows, axis=-1, keepdims=True) + EPS)
 
     def normed_slab(k):
-        slab = jnp.where(core == 0, z - 1 - k, z + k) % n_fs
+        slab = slab_of(k, core, z, n_fs)
         part = lax.dynamic_slice_in_dim(tokens, slab * LANES, LANES, axis=1).astype(jnp.float32)
         return (part * inverse * lax.dynamic_slice_in_dim(pre_gain, slab * LANES, LANES)).astype(low)
 

time: 235 us -> 244 us (1.038)
  waiting for transfers between devices: 21.2 us -> 55.3 us
  starting transfers between devices: 145 us -> 112 us
  blocking collectives: 48 us -> 56.4 us
    ppermute x21, starting transfers between devices: 112 us -> 40.9 us  [body(): held[chain] = lax.ppermute(held[chain], both, ring)]
    ppermute x1, starting transfers between devices: 5.17 us -> 45.1 us  [body(): other0 = lax.ppermute(packed, both, enter)]
    ppermute x21, waiting for transfers between devices: 19 us -> 53.1 us  [body(): held[chain] = lax.ppermute(held[chain], both, ring)]
    all_to_all x2, blocking collectives: 48 us -> 56.4 us  [over_chips(): lax.all_to_all(array, 'tp', 0, 0, axis_index_groups=chips, tiled=True)]
    ppermute x1, starting transfers between devices: 12.3 us -> 8.78 us  [body(): other = lax.ppermute(mine, 'tp', partner)]
  transfers between devices with their start and end apart: 25 -> 25, of which waited for: 10 -> 16; matrix products, arithmetic and copies ran while one was open for 4% -> 4% of each run, Pallas kernels for 0% -> 0%
where the time goes in v3:
time: 244 us; the launch traced here: 243 us
  starting transfers between devices  112 us (46%)
  blocking collectives  56.4 us (23%)
  waiting for transfers between devices  55.3 us (23%)
  matrix products  8.32 us (3%)
  other arithmetic  5.64 us (2%)
  Pallas kernels  4.52 us (2%)
    all_to_all x2, blocking collectives, over_chips(): lax.all_to_all(array, 'tp', 0, 0, axis_index_groups=chips, tiled=True)  56.4 us
    ppermute x21, waiting for transfers between devices, body(): held[chain] = lax.ppermute(held[chain], both, ring)  53.1 us
    ppermute x1, starting transfers between devices, body(): other0 = lax.ppermute(packed, both, enter)  45.1 us
    ppermute x21, starting transfers between devices, body(): held[chain] = lax.ppermute(held[chain], both, ring)  40.9 us
    ppermute x1, starting transfers between devices, body(): arrived = lax.ppermute(sums, 'tp', partner)  16.1 us
    ppermute x1, starting transfers between devices, body(): other = lax.ppermute(mine, 'tp', partner)  8.78 us
    dot_general x16, matrix products, product(): lax.dot_general(weights, k_normed, (((1,), (1,)), ((), ())), preferred_el...  7.32 us
  transfers between devices with their start and end apart: 25, of which 16 were waited for; matrix products, arithmetic and copies ran while one was open for 4% of the time, Pallas kernels for 0%

profile of v3, /device:TPU:65, one launch (start us, length us, event | category | flops | bytes accessed | tf_op | source)
XLA Modules:
  0.0 243.0 jit_solution(6304149286187536170)
XLA Ops:
  0.0 0.9 convert_element_type.80
  0.9 1.2 fusion.5
  2.2 45.1 %collective-permute-start.8 = (bf16[1056,128]{1,0:T(8,128)(2,1)S(1)}, bf16[1056,128]{1,0:T(8,128)(2,1)S(1)}, u32[]{:S(2)}, u32[]{:S(2)}) collective-permute-start(bf16[1056,128]{1,0:T(8,128)(2,1)S(1)} %pad_maximum_fusion.1), channel_id=1, source_target_pairs={{0,1},{1,240},{2,3},{3,242},{4,5},{5,244},{6,7},{7,246},{8,9},{9,2... | collective-permute-start | bytes 811016 | tf_op jit(solution)/shard_map/ppermute | solution.py:112
  47.2 0.7 collective-permute-start
  47.9 2.1 multiply_reduce_fusion
  50.2 2.1 collective-permute-start.1
  52.5 2.0 collective-permute-start.9
  54.5 2.0 collective-permute-start.17
  56.5 1.4 collective-permute-done.1
  58.8 1.2 collective-permute-done.9
  60.4 2.0 collective-permute-start.10
  62.4 2.0 collective-permute-start.2
  64.8 3.1 %collective-permute-done.10 = bf16[704,128]{1,0:T(8,128)(2,1)S(1)} collective-permute-done((bf16[704,128]{1,0:T(8,128)(2,1)S(1)}, bf16[704,128]{1,0:T(8,128)(2,1)S(1)}, u32[]{:S(2)}, u32[]{:S(2)}) %collective-permute-start.10) | collective-permute-done | bytes 180256 | tf_op jit(solution)/shard_map/ppermute | solution.py:139
  67.9 1.9 collective-permute-start.11
  69.8 1.9 collective-permute-start.3
  72.7 2.6 %collective-permute-done.11 = bf16[704,128]{1,0:T(8,128)(2,1)S(1)} collective-permute-done((bf16[704,128]{1,0:T(8,128)(2,1)S(1)}, bf16[704,128]{1,0:T(8,128)(2,1)S(1)}, u32[]{:S(2)}, u32[]{:S(2)}) %collective-permute-start.11) | collective-permute-done | bytes 180256 | tf_op jit(solution)/shard_map/ppermute | solution.py:139
  75.4 1.9 collective-permute-start.12
  77.3 1.9 collective-permute-start.4
  80.2 2.6 %collective-permute-done.12 = bf16[704,128]{1,0:T(8,128)(2,1)S(1)} collective-permute-done((bf16[704,128]{1,0:T(8,128)(2,1)S(1)}, bf16[704,128]{1,0:T(8,128)(2,1)S(1)}, u32[]{:S(2)}, u32[]{:S(2)}) %collective-permute-start.12) | collective-permute-done | bytes 180256 | tf_op jit(solution)/shard_map/ppermute | solution.py:139
  82.8 1.9 collective-permute-start.13
  84.8 1.9 collective-permute-start.5
  87.7 2.6 %collective-permute-done.13 = bf16[704,128]{1,0:T(8,128)(2,1)S(1)} collective-permute-done((bf16[704,128]{1,0:T(8,128)(2,1)S(1)}, bf16[704,128]{1,0:T(8,128)(2,1)S(1)}, u32[]{:S(2)}, u32[]{:S(2)}) %collective-permute-start.13) | collective-permute-done | bytes 180256 | tf_op jit(solution)/shard_map/ppermute | solution.py:139
  90.3 1.9 collective-permute-start.14
  92.3 1.9 collective-permute-start.6
  95.1 2.6 %collective-permute-done.14 = bf16[704,128]{1,0:T(8,128)(2,1)S(1)} collective-permute-done((bf16[704,128]{1,0:T(8,128)(2,1)S(1)}, bf16[704,128]{1,0:T(8,128)(2,1)S(1)}, u32[]{:S(2)}, u32[]{:S(2)}) %collective-permute-start.14) | collective-permute-done | bytes 180256 | tf_op jit(solution)/shard_map/ppermute | solution.py:139
  97.8 1.9 collective-permute-start.15
  99.7 1.9 collective-permute-start.7
  102.6 2.6 %collective-permute-done.15 = bf16[704,128]{1,0:T(8,128)(2,1)S(1)} collective-permute-done((bf16[704,128]{1,0:T(8,128)(2,1)S(1)}, bf16[704,128]{1,0:T(8,128)(2,1)S(1)}, u32[]{:S(2)}, u32[]{:S(2)}) %collective-permute-start.15) | collective-permute-done | bytes 180256 | tf_op jit(solution)/shard_map/ppermute | solution.py:139
  105.7 1.5 collective-permute-done.7
  107.8 16.1 %collective-permute-start.16 = (bf16[1408,512]{1,0:T(8,128)(2,1)S(1)}, bf16[1408,512]{1,0:T(8,128)(2,1)S(1)}, u32[]{:S(2)}, u32[]{:S(2)}) collective-permute-start(bf16[1408,512]{1,0:T(8,128)(2,1)S(1)} %pad_maximum_fusion), channel_id=1, source_target_pairs={{0,1},{1,0},{2,3},{3,2},{4,5},{5,4},{6,7},{7,6},{8,9},{9,8},{10,11... | collective-permute-start | bytes 4325384 | tf_op jit(solution)/shard_map/ppermute | solution.py:146
  123.9 2.0 collective-permute-start.18
  125.9 5.5 %collective-permute-done.18 = bf16[704,128]{1,0:T(8,128)(2,1)S(1)} collective-permute-done((bf16[704,128]{1,0:T(8,128)(2,1)S(1)}, bf16[704,128]{1,0:T(8,128)(2,1)S(1)}, u32[]{:S(2)}, u32[]{:S(2)}) %collective-permute-start.18) | collective-permute-done | bytes 180256 | tf_op jit(solution)/shard_map/ppermute | solution.py:139
  131.4 1.9 collective-permute-start.19
  133.3 5.5 %collective-permute-done.19 = bf16[704,128]{1,0:T(8,128)(2,1)S(1)} collective-permute-done((bf16[704,128]{1,0:T(8,128)(2,1)S(1)}, bf16[704,128]{1,0:T(8,128)(2,1)S(1)}, u32[]{:S(2)}, u32[]{:S(2)}) %collective-permute-start.19) | collective-permute-done | bytes 180256 | tf_op jit(solution)/shard_map/ppermute | solution.py:139
  138.8 1.9 collective-permute-start.20
  140.8 5.5 %collective-permute-done.20 = bf16[704,128]{1,0:T(8,128)(2,1)S(1)} collective-permute-done((bf16[704,128]{1,0:T(8,128)(2,1)S(1)}, bf16[704,128]{1,0:T(8,128)(2,1)S(1)}, u32[]{:S(2)}, u32[]{:S(2)}) %collective-permute-start.20) | collective-permute-done | bytes 180256 | tf_op jit(solution)/shard_map/ppermute | solution.py:139
  146.3 1.9 collective-permute-start.21
  148.4 5.4 %collective-permute-done.21 = bf16[704,128]{1,0:T(8,128)(2,1)S(1)} collective-permute-done((bf16[704,128]{1,0:T(8,128)(2,1)S(1)}, bf16[704,128]{1,0:T(8,128)(2,1)S(1)}, u32[]{:S(2)}, u32[]{:S(2)}) %collective-permute-start.21) | collective-permute-done | bytes 180256 | tf_op jit(solution)/shard_map/ppermute | solution.py:139
  153.8 1.9 collective-permute-start.22
  155.9 5.4 %collective-permute-done.22 = bf16[704,128]{1,0:T(8,128)(2,1)S(1)} collective-permute-done((bf16[704,128]{1,0:T(8,128)(2,1)S(1)}, bf16[704,128]{1,0:T(8,128)(2,1)S(1)}, u32[]{:S(2)}, u32[]{:S(2)}) %collective-permute-start.22) | collective-permute-done | bytes 180256 | tf_op jit(solution)/shard_map/ppermute | solution.py:139
  161.3 1.9 collective-permute-start.23
  163.3 5.4 %collective-permute-done.23 = bf16[704,128]{1,0:T(8,128)(2,1)S(1)} collective-permute-done((bf16[704,128]{1,0:T(8,128)(2,1)S(1)}, bf16[704,128]{1,0:T(8,128)(2,1)S(1)}, u32[]{:S(2)}, u32[]{:S(2)}) %collective-permute-start.23) | collective-permute-done | bytes 180256 | tf_op jit(solution)/shard_map/ppermute | solution.py:139
  169.8 1.0 convolution_convert_fusion
  170.8 29.9 %all_to_all.10 = bf16[8,64,1024]{2,1,0:T(8,128)(2,1)S(1)} all-to-all(bf16[8,64,1024]{2,1,0:T(8,128)(2,1)S(1)} %bitcast.29), channel_id=1, replica_groups={{0,2,4,6,8,10,12,14},{1,3,5,7,9,11,13,15},{16,18,20,22,24,26,28,30},{17..., dimensions={0} | all-to-all | bytes 2097152 | tf_op jit(solution)/shard_map/all_to_all | solution.py:163
  201.0 26.4 %all_to_all.11 = bf16[8,64,1024]{2,1,0:T(8,128)(2,1)S(1)} all-to-all(bf16[8,64,1024]{2,1,0:T(8,128)(2,1)S(1)} %broadcast_in_dim.2), channel_id=1, replica_groups={{0,2,4,6,8,10,12,14},{1,3,5,7,9,11,13,15},{16,18,20,22,24,26,28,30},{17..., dimensions={0} | all-to-all | bytes 2097152 | tf_op jit(solution)/shard_map/all_to_all | solution.py:163
  227.4 8.8 %collective-permute-start.24 = (bf16[512,1024]{1,0:T(8,128)(2,1)S(1)}, bf16[512,1024]{1,0:T(8,128)(2,1)S(1)}, u32[]{:S(2)}, u32[]{:S(2)}) collective-permute-start(bf16[512,1024]{1,0:T(8,128)(2,1)S(1)} %bitcast.25), channel_id=1, source_target_pairs={{0,1},{1,0},{2,3},{3,2},{4,5},{5,4},{6,7},{7,6},{8,9},{9,8},{10,11... | collective-permute-start | bytes 3145736 | tf_op jit(solution)/shard_map/ppermute | solution.py:180
  236.3 2.2 collective-permute-done.24.refs_2_
  238.5 4.5 %shard_map.91 = bf16[512,2048]{1,0:T(8,128)(2,1)} custom-call(s32[2]{0:T(128)S(1)} %pad_add_fusion.refs_0_, bf16[512,1024]{1,0:T(8,128)(2,1)S(1)} %bitcast.26, bf16[512,1024]{1,0:T(8,128)(2,1)S(1)} %collective-permute-done.24.refs_2_, f32[16,128]{1,0:T(8,128)S(1)} %bitcast.27, f32[16,128]{1,0:T(8,128)S(1)} %bitcast.28), custom_call_target="tpu_custom_call" | custom-call | tf_op jit(solution)/shard_map/pallas_call | solution.py:68
  (56 shorter events, 9.6 us)
Async XLA Ops:
  2.2 50.2 %copy-start.3 = (f32[2048]{0:T(1024)S(1)}, f32[2048]{0:T(1024)}, u32[]{:S(2)}) copy-start(f32[2048]{0:T(1024)} %param.10) | copy-start | bytes 24580
  2.2 50.3 %collective-permute-start.8 = (bf16[1056,128]{1,0:T(8,128)(2,1)S(1)}, bf16[1056,128]{1,0:T(8,128)(2,1)S(1)}, u32[]{:S(2)}, u32[]{:S(2)}) collective-permute-start(bf16[1056,128]{1,0:T(8,128)(2,1)S(1)} %pad_maximum_fusion.1), channel_id=1, source_target_pairs={{0,1},{1,240},{2,3},{3,242},{4,5},{5,244},{6,7},{7,246},{8,9},{9,2... | collective-permute-start | bytes 811016 | tf_op jit(solution)/shard_map/ppermute | solution.py:112
  47.2 2.9 %collective-permute-start = (bf16[1056,128]{1,0:T(8,128)(2,1)S(1)}, bf16[1056,128]{1,0:T(8,128)(2,1)S(1)}, u32[]{:S(2)}, u32[]{:S(2)}) collective-permute-start(bf16[1056,128]{1,0:T(8,128)(2,1)S(1)} %pad_maximum_fusion.1), channel_id=1, source_target_pairs={{0,240},{2,242},{4,244},{6,246},{8,248},{10,250},{12,252},{14,254}... | collective-permute-start | bytes 811016 | tf_op jit(solution)/shard_map/ppermute | solution.py:113
  50.0 7.8 %copy-start.2 = (bf16[512,2048]{1,0:T(8,128)(2,1)S(1)}, bf16[512,2048]{1,0:T(8,128)(2,1)}, u32[]{:S(2)}) copy-start(bf16[512,2048]{1,0:T(8,128)(2,1)} %param.9) | copy-start | bytes 6291460
  50.2 7.6 %collective-permute-start.1 = (bf16[704,128]{1,0:T(8,128)(2,1)S(1)}, bf16[704,128]{1,0:T(8,128)(2,1)S(1)}, u32[]{:S(2)}, u32[]{:S(2)}) collective-permute-start(bf16[704,128]{1,0:T(8,128)(2,1)S(1)} %slice.40), channel_id=1, source_target_pairs={{0,240},{1,17},{2,242},{3,19},{4,244},{5,21},{6,246},{7,23},{8,248... | collective-permute-start | bytes 540680 | tf_op jit(solution)/shard_map/ppermute | solution.py:139
  52.5 7.5 %collective-permute-start.9 = (bf16[704,128]{1,0:T(8,128)(2,1)S(1)}, bf16[704,128]{1,0:T(8,128)(2,1)S(1)}, u32[]{:S(2)}, u32[]{:S(2)}) collective-permute-start(bf16[704,128]{1,0:T(8,128)(2,1)S(1)} %slice.41), channel_id=1, source_target_pairs={{0,240},{1,17},{2,242},{3,19},{4,244},{5,21},{6,246},{7,23},{8,248... | collective-permute-start | bytes 540680 | tf_op jit(solution)/shard_map/ppermute | solution.py:139
  54.5 69.4 %collective-permute-start.17 = (bf16[704,128]{1,0:T(8,128)(2,1)S(1)}, bf16[704,128]{1,0:T(8,128)(2,1)S(1)}, u32[]{:S(2)}, u32[]{:S(2)}) collective-permute-start(bf16[704,128]{1,0:T(8,128)(2,1)S(1)} %get-tuple-element.7), channel_id=1, source_target_pairs={{0,240},{1,17},{2,242},{3,19},{4,244},{5,21},{6,246},{7,23},{8,248... | collective-permute-start | bytes 540680 | tf_op jit(solution)/shard_map/ppermute | solution.py:139
  60.4 7.5 %collective-permute-start.10 = (bf16[704,128]{1,0:T(8,128)(2,1)S(1)}, bf16[704,128]{1,0:T(8,128)(2,1)S(1)}, u32[]{:S(2)}, u32[]{:S(2)}) collective-permute-start(bf16[704,128]{1,0:T(8,128)(2,1)S(1)} %collective-permute-done.9), channel_id=1, source_target_pairs={{0,240},{1,17},{2,242},{3,19},{4,244},{5,21},{6,246},{7,23},{8,248... | collective-permute-start | bytes 540680 | tf_op jit(solution)/shard_map/ppermute | solution.py:139
  62.4 7.5 %collective-permute-start.2 = (bf16[704,128]{1,0:T(8,128)(2,1)S(1)}, bf16[704,128]{1,0:T(8,128)(2,1)S(1)}, u32[]{:S(2)}, u32[]{:S(2)}) collective-permute-start(bf16[704,128]{1,0:T(8,128)(2,1)S(1)} %collective-permute-done.1), channel_id=1, source_target_pairs={{0,240},{1,17},{2,242},{3,19},{4,244},{5,21},{6,246},{7,23},{8,248... | collective-permute-start | bytes 540680 | tf_op jit(solution)/shard_map/ppermute | solution.py:139
  67.9 7.5 %collective-permute-start.11 = (bf16[704,128]{1,0:T(8,128)(2,1)S(1)}, bf16[704,128]{1,0:T(8,128)(2,1)S(1)}, u32[]{:S(2)}, u32[]{:S(2)}) collective-permute-start(bf16[704,128]{1,0:T(8,128)(2,1)S(1)} %collective-permute-done.10), channel_id=1, source_target_pairs={{0,240},{1,17},{2,242},{3,19},{4,244},{5,21},{6,246},{7,23},{8,248... | collective-permute-start | bytes 540680 | tf_op jit(solution)/shard_map/ppermute | solution.py:139
  69.8 7.5 %collective-permute-start.3 = (bf16[704,128]{1,0:T(8,128)(2,1)S(1)}, bf16[704,128]{1,0:T(8,128)(2,1)S(1)}, u32[]{:S(2)}, u32[]{:S(2)}) collective-permute-start(bf16[704,128]{1,0:T(8,128)(2,1)S(1)} %collective-permute-done.2), channel_id=1, source_target_pairs={{0,240},{1,17},{2,242},{3,19},{4,244},{5,21},{6,246},{7,23},{8,248... | collective-permute-start | bytes 540680 | tf_op jit(solution)/shard_map/ppermute | solution.py:139
  75.4 7.5 %collective-permute-start.12 = (bf16[704,128]{1,0:T(8,128)(2,1)S(1)}, bf16[704,128]{1,0:T(8,128)(2,1)S(1)}, u32[]{:S(2)}, u32[]{:S(2)}) collective-permute-start(bf16[704,128]{1,0:T(8,128)(2,1)S(1)} %collective-permute-done.11), channel_id=1, source_target_pairs={{0,240},{1,17},{2,242},{3,19},{4,244},{5,21},{6,246},{7,23},{8,248... | collective-permute-start | bytes 540680 | tf_op jit(solution)/shard_map/ppermute | solution.py:139
  77.3 7.5 %collective-permute-start.4 = (bf16[704,128]{1,0:T(8,128)(2,1)S(1)}, bf16[704,128]{1,0:T(8,128)(2,1)S(1)}, u32[]{:S(2)}, u32[]{:S(2)}) collective-permute-start(bf16[704,128]{1,0:T(8,128)(2,1)S(1)} %collective-permute-done.3), channel_id=1, source_target_pairs={{0,240},{1,17},{2,242},{3,19},{4,244},{5,21},{6,246},{7,23},{8,248... | collective-permute-start | bytes 540680 | tf_op jit(solution)/shard_map/ppermute | solution.py:139
  82.8 7.5 %collective-permute-start.13 = (bf16[704,128]{1,0:T(8,128)(2,1)S(1)}, bf16[704,128]{1,0:T(8,128)(2,1)S(1)}, u32[]{:S(2)}, u32[]{:S(2)}) collective-permute-start(bf16[704,128]{1,0:T(8,128)(2,1)S(1)} %collective-permute-done.12), channel_id=1, source_target_pairs={{0,240},{1,17},{2,242},{3,19},{4,244},{5,21},{6,246},{7,23},{8,248... | collective-permute-start | bytes 540680 | tf_op jit(solution)/shard_map/ppermute | solution.py:139
  84.8 7.5 %collective-permute-start.5 = (bf16[704,128]{1,0:T(8,128)(2,1)S(1)}, bf16[704,128]{1,0:T(8,128)(2,1)S(1)}, u32[]{:S(2)}, u32[]{:S(2)}) collective-permute-start(bf16[704,128]{1,0:T(8,128)(2,1)S(1)} %collective-permute-done.4), channel_id=1, source_target_pairs={{0,240},{1,17},{2,242},{3,19},{4,244},{5,21},{6,246},{7,23},{8,248... | collective-permute-start | bytes 540680 | tf_op jit(solution)/shard_map/ppermute | solution.py:139
  90.3 7.5 %collective-permute-start.14 = (bf16[704,128]{1,0:T(8,128)(2,1)S(1)}, bf16[704,128]{1,0:T(8,128)(2,1)S(1)}, u32[]{:S(2)}, u32[]{:S(2)}) collective-permute-start(bf16[704,128]{1,0:T(8,128)(2,1)S(1)} %collective-permute-done.13), channel_id=1, source_target_pairs={{0,240},{1,17},{2,242},{3,19},{4,244},{5,21},{6,246},{7,23},{8,248... | collective-permute-start | bytes 540680 | tf_op jit(solution)/shard_map/ppermute | solution.py:139
  92.3 7.5 %collective-permute-start.6 = (bf16[704,128]{1,0:T(8,128)(2,1)S(1)}, bf16[704,128]{1,0:T(8,128)(2,1)S(1)}, u32[]{:S(2)}, u32[]{:S(2)}) collective-permute-start(bf16[704,128]{1,0:T(8,128)(2,1)S(1)} %collective-permute-done.5), channel_id=1, source_target_pairs={{0,240},{1,17},{2,242},{3,19},{4,244},{5,21},{6,246},{7,23},{8,248... | collective-permute-start | bytes 540680 | tf_op jit(solution)/shard_map/ppermute | solution.py:139
  97.8 7.5 %collective-permute-start.15 = (bf16[704,128]{1,0:T(8,128)(2,1)S(1)}, bf16[704,128]{1,0:T(8,128)(2,1)S(1)}, u32[]{:S(2)}, u32[]{:S(2)}) collective-permute-start(bf16[704,128]{1,0:T(8,128)(2,1)S(1)} %collective-permute-done.14), channel_id=1, source_target_pairs={{0,240},{1,17},{2,242},{3,19},{4,244},{5,21},{6,246},{7,23},{8,248... | collective-permute-start | bytes 540680 | tf_op jit(solution)/shard_map/ppermute | solution.py:139
  99.7 7.5 %collective-permute-start.7 = (bf16[704,128]{1,0:T(8,128)(2,1)S(1)}, bf16[704,128]{1,0:T(8,128)(2,1)S(1)}, u32[]{:S(2)}, u32[]{:S(2)}) collective-permute-start(bf16[704,128]{1,0:T(8,128)(2,1)S(1)} %collective-permute-done.6), channel_id=1, source_target_pairs={{0,240},{1,17},{2,242},{3,19},{4,244},{5,21},{6,246},{7,23},{8,248... | collective-permute-start | bytes 540680 | tf_op jit(solution)/shard_map/ppermute | solution.py:139
  107.8 61.0 %collective-permute-start.16 = (bf16[1408,512]{1,0:T(8,128)(2,1)S(1)}, bf16[1408,512]{1,0:T(8,128)(2,1)S(1)}, u32[]{:S(2)}, u32[]{:S(2)}) collective-permute-start(bf16[1408,512]{1,0:T(8,128)(2,1)S(1)} %pad_maximum_fusion), channel_id=1, source_target_pairs={{0,1},{1,0},{2,3},{3,2},{4,5},{5,4},{6,7},{7,6},{8,9},{9,8},{10,11... | collective-permute-start | bytes 4325384 | tf_op jit(solution)/shard_map/ppermute | solution.py:146
  123.9 7.5 %collective-permute-start.18 = (bf16[704,128]{1,0:T(8,128)(2,1)S(1)}, bf16[704,128]{1,0:T(8,128)(2,1)S(1)}, u32[]{:S(2)}, u32[]{:S(2)}) collective-permute-start(bf16[704,128]{1,0:T(8,128)(2,1)S(1)} %collective-permute-done.17), channel_id=1, source_target_pairs={{0,240},{1,17},{2,242},{3,19},{4,244},{5,21},{6,246},{7,23},{8,248... | collective-permute-start | bytes 540680 | tf_op jit(solution)/shard_map/ppermute | solution.py:139
  131.4 7.5 %collective-permute-start.19 = (bf16[704,128]{1,0:T(8,128)(2,1)S(1)}, bf16[704,128]{1,0:T(8,128)(2,1)S(1)}, u32[]{:S(2)}, u32[]{:S(2)}) collective-permute-start(bf16[704,128]{1,0:T(8,128)(2,1)S(1)} %collective-permute-done.18), channel_id=1, source_target_pairs={{0,240},{1,17},{2,242},{3,19},{4,244},{5,21},{6,246},{7,23},{8,248... | collective-permute-start | bytes 540680 | tf_op jit(solution)/shard_map/ppermute | solution.py:139
  138.8 7.5 %collective-permute-start.20 = (bf16[704,128]{1,0:T(8,128)(2,1)S(1)}, bf16[704,128]{1,0:T(8,128)(2,1)S(1)}, u32[]{:S(2)}, u32[]{:S(2)}) collective-permute-start(bf16[704,128]{1,0:T(8,128)(2,1)S(1)} %collective-permute-done.19), channel_id=1, source_target_pairs={{0,240},{1,17},{2,242},{3,19},{4,244},{5,21},{6,246},{7,23},{8,248... | collective-permute-start | bytes 540680 | tf_op jit(solution)/shard_map/ppermute | solution.py:139
  146.3 7.5 %collective-permute-start.21 = (bf16[704,128]{1,0:T(8,128)(2,1)S(1)}, bf16[704,128]{1,0:T(8,128)(2,1)S(1)}, u32[]{:S(2)}, u32[]{:S(2)}) collective-permute-start(bf16[704,128]{1,0:T(8,128)(2,1)S(1)} %collective-permute-done.20), channel_id=1, source_target_pairs={{0,240},{1,17},{2,242},{3,19},{4,244},{5,21},{6,246},{7,23},{8,248... | collective-permute-start | bytes 540680 | tf_op jit(solution)/shard_map/ppermute | solution.py:139
  153.8 7.5 %collective-permute-start.22 = (bf16[704,128]{1,0:T(8,128)(2,1)S(1)}, bf16[704,128]{1,0:T(8,128)(2,1)S(1)}, u32[]{:S(2)}, u32[]{:S(2)}) collective-permute-start(bf16[704,128]{1,0:T(8,128)(2,1)S(1)} %collective-permute-done.21), channel_id=1, source_target_pairs={{0,240},{1,17},{2,242},{3,19},{4,244},{5,21},{6,246},{7,23},{8,248... | collective-permute-start | bytes 540680 | tf_op jit(solution)/shard_map/ppermute | solution.py:139
  161.3 7.5 %collective-permute-start.23 = (bf16[704,128]{1,0:T(8,128)(2,1)S(1)}, bf16[704,128]{1,0:T(8,128)(2,1)S(1)}, u32[]{:S(2)}, u32[]{:S(2)}) collective-permute-start(bf16[704,128]{1,0:T(8,128)(2,1)S(1)} %collective-permute-done.22), channel_id=1, source_target_pairs={{0,240},{1,17},{2,242},{3,19},{4,244},{5,21},{6,246},{7,23},{8,248... | collective-permute-start | bytes 540680 | tf_op jit(solution)/shard_map/ppermute | solution.py:139
  200.9 37.6 %copy-start = (f32[2048]{0:T(1024)S(1)}, f32[2048]{0:T(1024)}, u32[]{:S(2)}) copy-start(f32[2048]{0:T(1024)} %param.16) | copy-start | bytes 24580
  200.9 37.6 %copy-start.1 = (f32[2048]{0:T(1024)S(1)}, f32[2048]{0:T(1024)}, u32[]{:S(2)}) copy-start(f32[2048]{0:T(1024)} %param.17) | copy-start | bytes 24580
  227.4 11.1 %collective-permute-start.24 = (bf16[512,1024]{1,0:T(8,128)(2,1)S(1)}, bf16[512,1024]{1,0:T(8,128)(2,1)S(1)}, u32[]{:S(2)}, u32[]{:S(2)}) collective-permute-start(bf16[512,1024]{1,0:T(8,128)(2,1)S(1)} %bitcast.25), channel_id=1, source_target_pairs={{0,1},{1,0},{2,3},{3,2},{4,5},{5,4},{6,7},{7,6},{8,9},{9,8},{10,11... | collective-permute-start | bytes 3145736 | tf_op jit(solution)/shard_map/ppermute | solution.py:180
